TPU v7x, 32 devices: a whole 2x2x4 slice. The times are simulated.
32 devices in a mesh: ep: 8 (over z, y), tp: 4 (over x, core).
Axes of the slice: x: 2, y: 2, z: 4, core: 2. Of those that a mesh axis runs over, the one named last changes fastest.
Arguments:
- tokens: bfloat16 [192, 1024], P('ep'), may hold values from -1.796875 to 1.796875
- attn_gain: float32 [1024], replicated, may hold values from 0.1 to 1.9
- w_query: bfloat16 [1024, 1024], P(None, 'tp'), may hold values from -0.1875 to 0.1875
- w_key: bfloat16 [1024, 256], P(None, 'tp'), may hold values from -0.1875 to 0.1875
- w_value: bfloat16 [1024, 256], P(None, 'tp'), may hold values from -0.1875 to 0.1875
- w_forget: bfloat16 [1024, 4], P(None, 'tp'), may hold values from -0.1875 to 0.1875
- forget_bias: float32 [4], P('tp'), may hold values from -1 to 2
- query_gain: float32 [64], replicated, may hold values from 0.1 to 1.9
- key_gain: float32 [64], replicated, may hold values from 0.1 to 1.9
- cache_pairs: bfloat16 [192, 4, 1024, 128], P('ep', 'tp'), may hold values from -6 to 206
- cache_cum: float32 [192, 4, 1024], P('ep', 'tp'), may hold values from -1024 to 0, as said below
- lengths: int32 [192], P('ep'), may hold values from 64 to 1024, as said below
- w_output: bfloat16 [1024, 1024], P('tp'), may hold values from -0.1875 to 0.1875
- ffn_gain: float32 [1024], replicated, may hold values from 0.1 to 1.9
- expert_ids: int32 [192, 2], replicated, may hold values from 0 to 7, all different within a row; in each aligned block of 24 rows (0 to 23, 24 to 47, ...) at most 16 rows name the same one
- route_weight: float32 [192, 2], replicated, may hold values from 0.2 to 1
- w_exp_gate: bfloat16 [8, 1024, 3584], P('ep', None, 'tp'), may hold values from -0.1875 to 0.1875
- w_exp_up: bfloat16 [8, 1024, 3584], P('ep', None, 'tp'), may hold values from -0.1875 to 0.1875
- w_exp_down: bfloat16 [8, 3584, 1024], P('ep', 'tp'), may hold values from -0.09375 to 0.09375
- shared_gate: bfloat16 [1024], replicated, may hold values from -0.1875 to 0.1875
- w_dense_gate: bfloat16 [4096, 1024], P('ep'), may hold values from -0.1875 to 0.1875
- w_dense_up: bfloat16 [4096, 1024], P('ep'), may hold values from -0.1875 to 0.1875
- w_dense_down: bfloat16 [4096, 1024], P('ep', 'tp'), may hold values from -0.09375 to 0.09375
Outputs:
- layer_out: bfloat16 [192, 1024], P('ep', 'tp')
Inputs may be any that keep to these rules, and one draw needn't show every extreme that they name: The cache of sequence b holds positions 0 to lengths[b] - 1; some sequence has 1024. `expert_ids`: each row names 2 different experts; in each aligned block of 24 rows no expert is named by more than 16 rows. cache_cum[b, g, s] never rises with s.
All inputs are finite; a program needn't handle non-finite values.
Results may differ from a plain program's by a relative error of at most 0.02.
Values may be sent and summed in bfloat16 or wider, within the bound.
A program may use at most 64 MiB of HBM per device.

v0:
```python
import functools

import jax
import jax.numpy as jnp
from jax import lax
from jax.experimental import pallas as pl
from jax.experimental.pallas import tpu as pltpu
from jax.sharding import PartitionSpec as P

EPSILON = 1e-06
MESH = pl.DeviceIdType.MESH
VMEM_BYTES = 56 * 1024 * 1024


def whole_layer(
    n_ep, n_tp, cap,
    tokens_ref, attn_gain_ref, query_gain_ref, key_gain_ref, forget_ref, bias_ref, length_ref,
    gain_ref, ids_ref, route_ref, shared_ref,
    wq_hbm, wk_hbm, wv_hbm, cum_hbm, cache_hbm, wo_hbm,
    wg_hbm, wu_hbm, wd_hbm, dg_hbm, du_hbm, dd_hbm,
    out_ref,
    wq, wk, wv, cum, cache, wo_ref, mixed,
    wg, wu, wd, dg, du, dd,
    part_out, part_in, gathered, rows_f, exp_out, exp_in, total, sum_out, sum_in,
    attn_sem, load_sem, part_send, part_recv, ring_send, ring_recv, fan_send, fan_recv,
    exp_send, exp_recv, sum_send, sum_recv,
):
    me = lax.axis_index("ep")
    col = lax.axis_index("tp")
    seq_rows, width = tokens_ref.shape
    span = width // n_tp
    slots = n_ep * cap
    batch = n_ep * seq_rows
    f32 = jnp.float32
    head = query_gain_ref.shape[1]
    heads = wq.shape[1] // head
    bunch = 4
    small = [
        pltpu.make_async_copy(src, dst, attn_sem.at[i])
        for i, (src, dst) in enumerate(
            ((wq_hbm, wq), (wk_hbm, wk), (wv_hbm, wv), (cum_hbm.at[:, 0], cum), (wo_hbm, wo_ref)))
    ]
    caches = [
        pltpu.make_async_copy(cache_hbm.at[pl.ds(b, bunch), 0], cache.at[pl.ds(b, bunch)], attn_sem.at[5 + b // bunch])
        for b in range(0, seq_rows, bunch)
    ]
    for load in small[:4] + caches + small[4:]:
        load.start()
    loads = [
        pltpu.make_async_copy(src, dst, load_sem.at[i])
        for i, (src, dst) in enumerate(
            ((wg_hbm.at[0], wg), (wu_hbm.at[0], wu), (wd_hbm.at[0], wd),
             (dg_hbm, dg), (du_hbm, du), (dd_hbm, dd))
        )
    ]
    for load in loads:
        load.start()

    barrier = pltpu.get_barrier_semaphore()
    for k in range(1, n_ep):
        pl.semaphore_signal(barrier, inc=1, device_id={"ep": lax.rem(me + k, n_ep)}, device_id_type=MESH)
    for d in range(1, n_tp):
        pl.semaphore_signal(barrier, inc=1, device_id={"tp": lax.rem(col + d, n_tp)}, device_id_type=MESH)

    def columns(d):
        return pl.ds(pl.multiple_of(lax.rem(col + d, n_tp) * span, span), span)

    def to_tp(src, dst, send, recv, d):
        return pltpu.make_async_remote_copy(
            src_ref=src, dst_ref=dst, send_sem=send, recv_sem=recv,
            device_id={"tp": lax.rem(col + d, n_tp)}, device_id_type=MESH)

    def to_ep(src, dst, send, recv, k):
        return pltpu.make_async_remote_copy(
            src_ref=src, dst_ref=dst, send_sem=send, recv_sem=recv,
            device_id={"ep": lax.rem(me + k, n_ep)}, device_id_type=MESH)

    high = lax.Precision.HIGHEST
    contract = (((1,), (1,)), ((), ()))

    def iota(shape, axis):
        return lax.broadcasted_iota(jnp.int32, shape, axis).astype(f32)

    def group_of(values, size):
        return jnp.floor((values + 0.5) * (1.0 / size))

    def rms(values, gain):
        return values * lax.rsqrt(jnp.mean(values * values, axis=1, keepdims=True) + EPSILON) * gain

    lines = seq_rows * heads
    wide = heads * head
    token_f = tokens_ref[...].astype(f32)
    normed_one = rms(token_f, attn_gain_ref[...]).astype(jnp.bfloat16)
    gate_in = jnp.sum(normed_one.astype(f32) * forget_ref[...].astype(f32), axis=1, keepdims=True) + bias_ref[0]
    log_gate = jnp.minimum(gate_in, 0.0) - jnp.log(1.0 + jnp.exp(-jnp.abs(gate_in)))
    same_head = (group_of(iota((wide, wide), 0), head) == group_of(iota((wide, wide), 1), head)).astype(f32)
    spread = (group_of(iota((lines, seq_rows), 0), heads) == iota((lines, seq_rows), 1)).astype(f32)
    line_at = iota((lines, wide), 0)
    line_head = line_at - heads * group_of(line_at, heads)
    lane_head = group_of(iota((lines, wide), 1), head)
    own_head = line_head == lane_head
    fold_row = iota((wide, 2 * head), 0)
    fold = ((fold_row - head * group_of(fold_row, head)) == iota((wide, 2 * head), 1)).astype(jnp.bfloat16)
    widen_lane = iota((2 * head, wide), 1)
    widen = (iota((2 * head, wide), 0) - head == widen_lane - head * group_of(widen_lane, head)).astype(jnp.bfloat16)
    spread_b = spread.astype(jnp.bfloat16)
    eye = iota((seq_rows, seq_rows), 0) == iota((seq_rows, seq_rows), 1)
    lengths = jnp.sum(jnp.where(eye, jnp.broadcast_to(length_ref[...].astype(f32), (seq_rows, seq_rows)), 0.0), axis=1, keepdims=True)
    query_gain = jnp.concatenate([query_gain_ref[...]] * heads, axis=1)

    small[0].wait()
    query_raw = jnp.dot(normed_one, wq[...], preferred_element_type=f32)
    query_ms = jnp.dot(query_raw * query_raw, same_head, precision=high, preferred_element_type=f32) / head
    query = (query_raw * lax.rsqrt(query_ms + EPSILON) * query_gain).astype(jnp.bfloat16)
    small[1].wait()
    key = rms(lax.dot_general(normed_one, wk[...], contract, preferred_element_type=f32), key_gain_ref[...])
    small[2].wait()
    value = lax.dot_general(normed_one, wv[...], contract, preferred_element_type=f32)
    own_pair = jnp.concatenate([key, value], axis=1).astype(jnp.bfloat16)
    queries = jnp.dot(spread_b, query, preferred_element_type=f32)
    queries = jnp.where(own_head, queries, 0.0).astype(jnp.bfloat16)
    queries = jnp.dot(queries, fold, preferred_element_type=f32)
    pairs = jnp.dot(spread_b, own_pair, preferred_element_type=f32)
    multiplier = head ** (-0.5)
    own_score = jnp.sum(queries * pairs, axis=1, keepdims=True) * multiplier
    small[3].wait()
    position = iota(cum.shape, 1)
    now = jnp.sum(jnp.where(position == lengths - 1.0, cum[...], 0.0), axis=1, keepdims=True) + log_gate
    decay = jnp.where(position < lengths, now - cum[...], -1e30)
    decay = jnp.dot(spread, decay, precision=high, preferred_element_type=f32)
    rows = bunch * heads
    row_seq = group_of(iota((rows, 2 * head), 0), heads)
    for i, load in enumerate(caches):
        load.wait()
        block = jnp.concatenate([cache[i * bunch + b] for b in range(bunch)], axis=1)
        lines_here = slice(i * rows, (i + 1) * rows)
        query_here = queries[lines_here]
        lhs = jnp.concatenate([jnp.where(row_seq == b, query_here, 0.0) for b in range(bunch)], axis=1).astype(jnp.bfloat16)
        score = lax.dot_general(lhs, block, (((1,), (1,)), ((), ())), preferred_element_type=f32) * multiplier
        score = score + decay[lines_here]
        own = own_score[lines_here]
        peak = jnp.maximum(jnp.max(score, axis=1, keepdims=True), own)
        past = jnp.exp(score - peak)
        own = jnp.exp(own - peak)
        denom = jnp.sum(past, axis=1, keepdims=True) + own
        prob = (past / denom).astype(jnp.bfloat16)
        own = (own / denom).astype(jnp.bfloat16).astype(f32)
        wide_mix = jnp.dot(prob, block, preferred_element_type=f32)
        mix = own * pairs[lines_here]
        for b in range(bunch):
            mix = mix + jnp.where(row_seq == b, wide_mix[:, 2 * head * b:2 * head * (b + 1)], 0.0)
        mixed[lines_here, :] = mix
    widened = jnp.dot(mixed[...].astype(jnp.bfloat16), widen, preferred_element_type=f32)
    widened = jnp.where(own_head, widened, 0.0).astype(jnp.bfloat16)
    gather_rows = (iota((seq_rows, lines), 0) == group_of(iota((seq_rows, lines), 1), heads)).astype(jnp.bfloat16)
    head_mix = jnp.dot(gather_rows, widened, preferred_element_type=f32).astype(jnp.bfloat16)
    small[4].wait()

    for d in range(1, n_tp):
        part_out[d] = jnp.dot(head_mix, wo_ref[:, columns(d)], preferred_element_type=f32).astype(jnp.bfloat16)
    pl.semaphore_wait(barrier, n_ep + n_tp - 2)
    parts = [to_tp(part_out.at[d], part_in.at[d], part_send.at[d], part_recv.at[d], d) for d in range(1, n_tp)]
    for copy in parts:
        copy.start()
    own = jnp.dot(head_mix, wo_ref[:, columns(0)], preferred_element_type=f32)
    attn = own.astype(jnp.bfloat16).astype(f32)
    token_block = tokens_ref[:, columns(0)].astype(f32)
    for copy in parts:
        copy.wait_recv()
    for d in range(1, n_tp):
        attn = attn + part_in[d].astype(f32)
    residual = (token_block + attn).astype(jnp.bfloat16)
    gathered[col, me] = residual

    rings = [to_ep(gathered.at[col, me], gathered.at[col, me], ring_send.at[k], ring_recv.at[k], k) for k in range(1, n_ep)]
    for copy in rings:
        copy.start()
    fans = []
    if n_tp == 4:
        beside = col + 1 - 2 * lax.rem(col, 2)
        across = lax.rem(col + 2, 4)
        routes, first = ((col, across), (col, beside), (across, beside)), 2
    else:
        routes, first = tuple((col, lax.rem(col + d, n_tp)) for d in range(1, n_tp)), n_tp - 1

    def fan_copies(k, slot):
        return [
            pltpu.make_async_remote_copy(
                src_ref=gathered.at[block, slot], dst_ref=gathered.at[block, slot],
                send_sem=fan_send.at[k, d], recv_sem=fan_recv.at[k, d],
                device_id={"tp": target}, device_id_type=MESH)
            for d, (block, target) in enumerate(routes)
        ]

    for k in range(n_ep):
        if k > 0:
            rings[k - 1].wait_recv()
        slot = lax.rem(me - k + n_ep, n_ep)
        fan = fan_copies(k, slot)
        for copy in fan[:first]:
            copy.start()
        fans.append(fan)

    expert = me
    hit = jnp.zeros((1, batch), f32)
    weight_row = jnp.zeros((1, batch), f32)
    for k in range(ids_ref.shape[0]):
        same = ids_ref[k:k + 1, :] == expert
        hit = hit + jnp.where(same, 1.0, 0.0)
        weight_row = weight_row + jnp.where(same, route_ref[k:k + 1, :], 0.0)
    row_at = iota((batch, batch), 0)
    col_at = iota((batch, batch), 1)
    before = (row_at <= col_at) & (row_at >= group_of(col_at, seq_rows) * seq_rows)
    hits = jnp.broadcast_to(hit, (8, batch))
    rank = jnp.dot(hits.astype(jnp.bfloat16), before.astype(f32).astype(jnp.bfloat16), preferred_element_type=f32)[0:1]
    slot_of = jnp.where((hit > 0.5) & (rank < cap + 0.5), group_of(iota((1, batch), 1), seq_rows) * cap + rank - 1.0, -1.0)
    pick_f = jnp.where(iota((slots, batch), 0) == slot_of, 1.0, 0.0)
    pick = pick_f.astype(jnp.bfloat16)
    place = pick_f.T.astype(jnp.bfloat16)
    weight = jnp.sum((pick_f * weight_row).T, axis=1, keepdims=True)

    for k in range(n_ep + 1):
        if k < n_ep and first < len(routes):
            fans[k][0].wait_recv()
            fans[k][2].start()
        k = k - 1
        if k < 0:
            continue
        for copy in (fans[k][1:] if first < len(routes) else fans[k]):
            copy.wait_recv()
        slot = lax.rem(me - k + n_ep, n_ep)
        blocks = [gathered[t, slot].astype(f32) for t in range(n_tp)]
        squares = sum(jnp.sum(b * b, axis=1, keepdims=True) for b in blocks)
        scale = lax.rsqrt(squares / width + EPSILON)
        for t in range(n_tp):
            rows_f[pl.ds(pl.multiple_of(slot * seq_rows, 8), seq_rows), t * span:(t + 1) * span] = (
                blocks[t] * scale * gain_ref[:, t * span:(t + 1) * span])
    normed = rows_f[...].astype(jnp.bfloat16)

    picked = jnp.dot(pick, normed, preferred_element_type=f32).astype(jnp.bfloat16)
    for load in loads[:3]:
        load.wait()
    gate = jnp.dot(picked, wg[...], preferred_element_type=f32)
    up = jnp.dot(picked, wu[...], preferred_element_type=f32)
    hidden = (gate / (1.0 + jnp.exp(-gate)) * up).astype(jnp.bfloat16)
    moves = []
    for d in sorted(range(1, n_tp), key=lambda d: d != 2):
        exp_out[d] = jnp.dot(hidden, wd[:, columns(d)], preferred_element_type=f32).astype(jnp.bfloat16)
        copy = to_tp(exp_out.at[d], exp_in.at[d], exp_send.at[d], exp_recv.at[d], d)
        copy.start()
        moves.append(copy)
    expert_rows = jnp.dot(hidden, wd[:, columns(0)], preferred_element_type=f32).astype(jnp.bfloat16).astype(f32)

    shared_tiles = shared_ref[...].astype(f32)
    shared = jnp.concatenate([shared_tiles[i:i + 1] for i in range(width // 128)], axis=1)
    for load in loads[3:]:
        load.wait()
    step = seq_rows * 8 if n_ep % 8 == 0 else batch

    def dense(at):
        rows = rows_f[pl.ds(at, step), :].astype(jnp.bfloat16)
        gate = lax.dot_general(rows, dg[...], contract, preferred_element_type=f32)
        up = lax.dot_general(rows, du[...], contract, preferred_element_type=f32)
        hidden = (gate / (1.0 + jnp.exp(-gate)) * up).astype(jnp.bfloat16)
        mix = jnp.sum(rows.astype(f32) * shared, axis=1, keepdims=True)
        mix = 1.0 / (1.0 + jnp.exp(-mix))
        total[pl.ds(at, step), :] = mix * jnp.dot(hidden, dd[...], preferred_element_type=f32)

    if step == batch:
        dense(0)
    else:
        @pl.loop(0, batch // step)
        def _(i):
            dense(pl.multiple_of(i * step, step))

    for copy in moves:
        copy.wait_recv()
    for d in range(1, n_tp):
        expert_rows = expert_rows + exp_in[d].astype(f32)
    placed = jnp.dot(place, expert_rows.astype(jnp.bfloat16), preferred_element_type=f32)
    total[...] = total[...] + placed * weight

    sums = []
    for k in range(1, n_ep):
        slot = lax.rem(me + k, n_ep)
        sum_out[k] = total[pl.ds(pl.multiple_of(slot * seq_rows, 8), seq_rows), :].astype(jnp.bfloat16)
        copy = to_ep(sum_out.at[k], sum_in.at[k], sum_send.at[k], sum_recv.at[k], k)
        copy.start()
        sums.append(copy)
    result = residual.astype(f32) + total[pl.ds(pl.multiple_of(me * seq_rows, 8), seq_rows), :]
    for k in range(1, n_ep):
        sums[k - 1].wait_recv()
        result = result + sum_in[k].astype(f32)
    out_ref[...] = result.astype(jnp.bfloat16)
    for copy in parts + rings + [c for fan in fans for c in fan] + moves + sums:
        copy.wait_send()


def layer_call(tokens, attn_gain, w_query, w_key, w_value, w_forget, forget_bias, query_gain, key_gain,
              cache_pairs, cache_cum, lengths, w_output, ffn_gain, expert_ids, route_weight, shared_gate,
              w_exp_gate, w_exp_up, w_exp_down, w_dense_gate, w_dense_up, w_dense_down):
    n_ep, n_tp = lax.axis_size("ep"), lax.axis_size("tp")
    seq_rows, width = tokens.shape
    cap = max(2, min(seq_rows, 128 // n_ep))
    span = width // n_tp
    slots, batch = n_ep * cap, n_ep * seq_rows
    bf16, f32 = jnp.bfloat16, jnp.float32
    vmem = pl.BlockSpec(memory_space=pltpu.VMEM)
    hbm = pl.BlockSpec(memory_space=pltpu.HBM)
    dma = pltpu.SemaphoreType.DMA
    return pl.pallas_call(
        functools.partial(whole_layer, n_ep, n_tp, cap),
        out_shape=jax.ShapeDtypeStruct((seq_rows, span), bf16),
        in_specs=[vmem] * 5 + [pl.BlockSpec(memory_space=pltpu.SMEM)] + [vmem] * 5 + [hbm] * 12,
        out_specs=vmem,
        scratch_shapes=[
            pltpu.VMEM(w_query.shape, bf16),
            pltpu.VMEM(w_key.shape[::-1], bf16),
            pltpu.VMEM(w_value.shape[::-1], bf16),
            pltpu.VMEM((seq_rows, cache_cum.shape[2]), f32),
            pltpu.VMEM((seq_rows,) + cache_pairs.shape[2:], bf16),
            pltpu.VMEM(w_output.shape, bf16),
            pltpu.VMEM((seq_rows * w_query.shape[1] // query_gain.shape[0], cache_pairs.shape[3]), f32),
            pltpu.VMEM(w_exp_gate.shape[1:], bf16),
            pltpu.VMEM(w_exp_up.shape[1:], bf16),
            pltpu.VMEM(w_exp_down.shape[1:], bf16),
            pltpu.VMEM(w_dense_gate.shape, bf16),
            pltpu.VMEM(w_dense_up.shape, bf16),
            pltpu.VMEM(w_dense_down.shape, bf16),
            pltpu.VMEM((n_tp, seq_rows, span), bf16),
            pltpu.VMEM((n_tp, seq_rows, span), bf16),
            pltpu.VMEM((n_tp, n_ep, seq_rows, span), bf16),
            pltpu.VMEM((batch, width), f32),
            pltpu.VMEM((n_tp, slots, span), bf16),
            pltpu.VMEM((n_tp, slots, span), bf16),
            pltpu.VMEM((batch, span), f32),
            pltpu.VMEM((n_ep, seq_rows, span), bf16),
            pltpu.VMEM((n_ep, seq_rows, span), bf16),
            dma((5 + seq_rows // 4,)),
            dma((6,)),
            dma((n_tp,)), dma((n_tp,)),
            dma((n_ep,)), dma((n_ep,)),
            dma((n_ep, n_tp)), dma((n_ep, n_tp)),
            dma((n_tp,)), dma((n_tp,)),
            dma((n_ep,)), dma((n_ep,)),
        ],
        compiler_params=pltpu.CompilerParams(
            collective_id=0, has_side_effects=True, vmem_limit_bytes=VMEM_BYTES),
        name="whole_layer",
    )(tokens, attn_gain.reshape(1, width), query_gain.reshape(1, -1), key_gain.reshape(1, -1),
      w_forget.reshape(1, width), forget_bias, lengths.reshape(1, seq_rows),
      ffn_gain.reshape(1, width), expert_ids.T, route_weight.T, shared_gate.reshape(width // 128, 128),
      w_query, w_key.T, w_value.T, cache_cum, cache_pairs, w_output,
      w_exp_gate, w_exp_up, w_exp_down,
      w_dense_gate, w_dense_up, w_dense_down)


def shards(
    tokens,
    attn_gain,
    w_query,
    w_key,
    w_value,
    w_forget,
    forget_bias,
    query_gain,
    key_gain,
    cache_pairs,
    cache_cum,
    lengths,
    w_output,
    ffn_gain,
    expert_ids,
    route_weight,
    w_exp_gate,
    w_exp_up,
    w_exp_down,
    shared_gate,
    w_dense_gate,
    w_dense_up,
    w_dense_down,
):
    return layer_call(
        tokens, attn_gain, w_query, w_key, w_value, w_forget, forget_bias, query_gain, key_gain,
        cache_pairs, cache_cum, lengths, w_output, ffn_gain, expert_ids, route_weight, shared_gate,
        w_exp_gate, w_exp_up, w_exp_down, w_dense_gate, w_dense_up, w_dense_down,
    )


def solution(mesh):
    in_specs = (
        P("ep", None),
        P(),
        P(None, "tp"),
        P(None, "tp"),
        P(None, "tp"),
        P(None, "tp"),
        P("tp"),
        P(),
        P(),
        P("ep", "tp", None, None),
        P("ep", "tp", None),
        P("ep"),
        P("tp", None),
        P(),
        P(),
        P(),
        P("ep", None, "tp"),
        P("ep", None, "tp"),
        P("ep", "tp", None),
        P(),
        P("ep", None),
        P("ep", None),
        P("ep", "tp"),
    )
    out_specs = P("ep", "tp")
    return jax.shard_map(shards, mesh=mesh, in_specs=in_specs, out_specs=out_specs, check_vma=False)
```

profile of v0, /device:TPU:0, one launch (start us, length us, event | category | flops | bytes accessed | tf_op | source)
XLA Modules:
  0.0 38.7 jit_solution(18420645031847860684)
XLA Ops:
  0.7 36.7 %whole_layer.1 = bf16[24,256]{1,0:T(8,128)(2,1)} custom-call(bf16[24,1024]{1,0:T(8,128)(2,1)} %tokens_ref.1, f32[1,1024]{1,0:T(1,128)} %bitcast.13, f32[1,64]{1,0:T(1,128)} %bitcast.19, f32[1,64]{1,0:T(1,128)} %bitcast.20, bf16[1,1024]{1,0:T(2,128)(2,1)} %bitcast.14, f32[1]{0:T(128)S(6)} %copy.25.bias_ref, s32[1,24]{1,0:T(1,128)} %bitcast.21, ...), custom_call_target="tpu_custom_call" | custom-call | tf_op jit(solution)/shard_map/whole_layer/pallas_call | solution.py:311
  37.4 1.3 %copy.26 = bf16[24,256]{1,0:T(8,128)(2,1)} copy(bf16[24,256]{1,0:T(8,128)(2,1)} %whole_layer.1) | data formatting | bytes 24576
where the time goes:
time: 38.9 us; the launch traced here: 38.7 us
  Pallas kernels  36.7 us (94%)
  local copies, waits for them, and re-layouts  1.31 us (3%)
  between operations  0.66 us (2%)
    pallas_call x1, Pallas kernels, layer_call(): pl.pallas_call(functools.partial(whole_layer, n_ep, n_tp, cap), out_shape...  36.7 us
    unnamed x1, local copies, waits for them, and re-layouts  1.31 us

commit v1 on v0

v1 whole, which is shorter than its diff:
```python
import functools

import jax
import jax.numpy as jnp
from jax import lax
from jax.experimental import pallas as pl
from jax.experimental.pallas import tpu as pltpu
from jax.sharding import PartitionSpec as P

EPSILON = 1e-06
MESH = pl.DeviceIdType.MESH
VMEM_BYTES = 56 * 1024 * 1024


def whole_layer(
    n_ep, n_tp, cap,
    tokens_hbm, attn_gain_hbm, query_gain_hbm, key_gain_hbm, forget_hbm, bias_hbm, length_hbm,
    gain_hbm, ids_hbm, route_hbm, shared_hbm,
    wq_hbm, wk_hbm, wv_hbm, cum_hbm, cache_hbm, wo_hbm,
    wg_hbm, wu_hbm, wd_hbm, dg_hbm, du_hbm, dd_hbm,
    out_ref,
    tokens_ref, attn_gain_ref, query_gain_ref, key_gain_ref, forget_ref, bias_ref, length_ref,
    gain_ref, ids_ref, route_ref, shared_ref,
    wq, wkv, cum, cache, wo_ref, mixed,
    wg, wu, wd, dg, du, dd,
    part_out, part_in, gathered, rows_f, exp_out, exp_in, total, sum_out, sum_in,
    small_sem, attn_sem, load_sem, part_send, part_recv, ring_send, ring_recv, fan_send, fan_recv,
    exp_send, exp_recv, sum_send, sum_recv,
):
    me = lax.axis_index("ep")
    col = lax.axis_index("tp")
    seq_rows, width = tokens_ref.shape
    span = width // n_tp
    slots = n_ep * cap
    batch = n_ep * seq_rows
    f32, bf16 = jnp.float32, jnp.bfloat16
    head = query_gain_ref.shape[1]
    heads = wq.shape[1] // head
    lanes = 2 * head
    eight = 8
    bunch = 4
    small = [
        pltpu.make_async_copy(src, dst, small_sem.at[i])
        for i, (src, dst) in enumerate((
            (tokens_hbm, tokens_ref), (attn_gain_hbm, attn_gain_ref), (wq_hbm, wq),
            (wk_hbm, wkv.at[pl.ds(0, head)]), (wv_hbm, wkv.at[pl.ds(head, head)]),
            (forget_hbm, forget_ref), (bias_hbm, bias_ref), (length_hbm, length_ref),
            (query_gain_hbm, query_gain_ref), (key_gain_hbm, key_gain_ref), (cum_hbm.at[:, 0], cum)))
    ]
    caches = [
        pltpu.make_async_copy(cache_hbm.at[pl.ds(b, bunch), 0], cache.at[pl.ds(b, bunch)], attn_sem.at[b // bunch])
        for b in range(0, seq_rows, bunch)
    ]
    later = [
        pltpu.make_async_copy(src, dst, load_sem.at[i])
        for i, (src, dst) in enumerate((
            (wo_hbm, wo_ref), (gain_hbm, gain_ref), (ids_hbm, ids_ref), (route_hbm, route_ref),
            (shared_hbm, shared_ref), (wg_hbm.at[0], wg), (wu_hbm.at[0], wu), (wd_hbm.at[0], wd),
            (dg_hbm, dg), (du_hbm, du), (dd_hbm, dd)))
    ]
    for load in small + caches + later[:5]:
        load.start()

    barrier = pltpu.get_barrier_semaphore()
    for k in range(1, n_ep):
        pl.semaphore_signal(barrier, inc=1, device_id={"ep": lax.rem(me + k, n_ep)}, device_id_type=MESH)
    for d in range(1, n_tp):
        pl.semaphore_signal(barrier, inc=1, device_id={"tp": lax.rem(col + d, n_tp)}, device_id_type=MESH)

    def columns(d):
        return pl.ds(pl.multiple_of(lax.rem(col + d, n_tp) * span, span), span)

    def to_tp(src, dst, send, recv, d):
        return pltpu.make_async_remote_copy(
            src_ref=src, dst_ref=dst, send_sem=send, recv_sem=recv,
            device_id={"tp": lax.rem(col + d, n_tp)}, device_id_type=MESH)

    def to_ep(src, dst, send, recv, peer):
        return pltpu.make_async_remote_copy(
            src_ref=src, dst_ref=dst, send_sem=send, recv_sem=recv,
            device_id={"ep": peer}, device_id_type=MESH)

    if n_ep == 8:
        deep, side = me // 2, lax.rem(me, 2)
        low = (deep < 2).astype(jnp.int32)
        inner = low * deep + (1 - low) * (3 - deep)
        line = [inner, 1 - inner, 2, 3]
        line = [low * at + (1 - low) * (3 - at) for at in line]
        peers = [line[k // 2] * 2 + (side if k % 2 == 0 else 1 - side) for k in range(n_ep)]
    else:
        peers = [lax.rem(me + k, n_ep) for k in range(n_ep)]
    far_first = list(range(n_ep - 1, 0, -1))

    contract = (((1,), (1,)), ((), ()))

    def iota(shape, axis):
        return lax.broadcasted_iota(jnp.int32, shape, axis).astype(f32)

    def group_of(values, size):
        return jnp.floor((values + 0.5) * (1.0 / size))

    def rms(values, gain):
        return values * lax.rsqrt(jnp.mean(values * values, axis=1, keepdims=True) + EPSILON) * gain

    def rounded(values):
        return values.astype(bf16).astype(f32)

    def half_turn(values):
        return pltpu.roll(values, head, 1)

    left = lax.broadcasted_iota(jnp.int32, (seq_rows, lanes), 1) < head
    small[0].wait()
    small[1].wait()
    token_f = tokens_ref[...].astype(f32)
    normed_one = rms(token_f, attn_gain_ref[...]).astype(bf16)
    small[2].wait()
    query_raw = jnp.dot(normed_one, wq[...], preferred_element_type=f32)
    for load in small[3:10]:
        load.wait()
    pair_raw = lax.dot_general(normed_one, wkv[...], contract, preferred_element_type=f32)
    gate_in = jnp.sum(normed_one.astype(f32) * forget_ref[...].astype(f32), axis=1, keepdims=True) + bias_ref[...]
    log_gate = jnp.minimum(gate_in, 0.0) - jnp.log(1.0 + jnp.exp(-jnp.abs(gate_in)))
    eye = iota((seq_rows, seq_rows), 0) == iota((seq_rows, seq_rows), 1)
    lengths = jnp.sum(jnp.where(eye, jnp.broadcast_to(length_ref[...].astype(f32), (seq_rows, seq_rows)), 0.0), axis=1, keepdims=True)

    def half_scales(values):
        squares = values * values
        first = jnp.sum(jnp.where(left, squares, 0.0), axis=1, keepdims=True)
        second = jnp.sum(jnp.where(left, 0.0, squares), axis=1, keepdims=True)
        return lax.rsqrt(first / head + EPSILON), lax.rsqrt(second / head + EPSILON)

    gain_twice = jnp.concatenate([query_gain_ref[...]] * 2, axis=1)
    queries = []
    for a in range(heads // 2):
        raw = query_raw[:, lanes * a:lanes * (a + 1)]
        first, second = half_scales(raw)
        query = rounded(raw * jnp.where(left, first, second) * gain_twice)
        turned = half_turn(query)
        queries += [jnp.where(left, query, turned), jnp.where(left, turned, query)]
    key_scale, _ = half_scales(pair_raw)
    key_gain = jnp.concatenate([key_gain_ref[...]] * 2, axis=1)
    key = jnp.where(left, rounded(pair_raw * key_scale * key_gain), 0.0)
    value = rounded(pair_raw)
    value = jnp.where(left, half_turn(value), value)
    multiplier = head ** (-0.5)
    own_scores = [jnp.sum(query * key, axis=1, keepdims=True) * multiplier for query in queries]
    scaled = [query * multiplier for query in queries]
    small[10].wait()
    position = iota(cum.shape, 1)
    now = jnp.sum(jnp.where(position == lengths - 1.0, cum[...], 0.0), axis=1, keepdims=True) + log_gate
    cum[...] = jnp.where(position < lengths, now - cum[...], -1e30)

    row = lax.broadcasted_iota(jnp.int32, (eight, lanes), 0)
    left_eight = lax.broadcasted_iota(jnp.int32, (eight, lanes), 1) < head
    key_at = [row == jnp.where(left_eight, 2 * p, 2 * p + 1) for p in range(eight // 2)]
    value_at = [row == jnp.where(left_eight, 2 * p + 1, 2 * p) for p in range(eight // 2)]

    def score_of(i):
        lines = slice(i * eight, (i + 1) * eight)
        lhs = jnp.concatenate([
            jnp.concatenate([jnp.where(key_at[p], query[lines], 0.0) for query in scaled], axis=0)
            for p in range(eight // 2)], axis=1).astype(bf16)
        keys = jnp.concatenate([cache[i * eight + b, :, 0:head] for b in range(eight)], axis=1)
        return lax.dot_general(lhs, keys, contract, preferred_element_type=f32)

    def attend(i, score):
        lines = slice(i * eight, (i + 1) * eight)
        score = score + jnp.concatenate([cum[lines, :]] * heads, axis=0)
        own = jnp.concatenate([values[lines] for values in own_scores], axis=0)
        peak = jnp.maximum(jnp.max(score, axis=1, keepdims=True), own)
        past = jnp.exp(score - peak)
        own = jnp.exp(own - peak)
        inverse = 1.0 / (jnp.sum(past, axis=1, keepdims=True) + own)
        prob = (past * inverse).astype(bf16)
        own = rounded(own * inverse)
        values = jnp.concatenate([cache[i * eight + (b ^ 1), :, head:2 * head] for b in range(eight)], axis=1)
        wide = jnp.dot(prob, values, preferred_element_type=f32)
        mixes = []
        for h in range(heads):
            here = slice(h * eight, (h + 1) * eight)
            mix = sum(jnp.where(value_at[p], wide[here, lanes * p:lanes * (p + 1)], 0.0) for p in range(eight // 2))
            mixes.append(mix + half_turn(mix) + own[here] * value[lines])
        for a in range(heads // 2):
            mixed[lines, lanes * a:lanes * (a + 1)] = jnp.where(left_eight, mixes[2 * a], mixes[2 * a + 1])

    score = None
    for i in range(seq_rows // eight):
        for load in caches[i * eight // bunch:(i + 1) * eight // bunch]:
            load.wait()
        ahead = score_of(i)
        if score is not None:
            attend(i - 1, score)
        score = ahead
    for load in later[5:]:
        load.start()
    attend(seq_rows // eight - 1, score)
    head_mix = mixed[...].astype(bf16)
    later[0].wait()

    for d in range(1, n_tp):
        part_out[d] = jnp.dot(head_mix, wo_ref[:, columns(d)], preferred_element_type=f32).astype(bf16)
    pl.semaphore_wait(barrier, n_ep + n_tp - 2)
    parts = [to_tp(part_out.at[d], part_in.at[d], part_send.at[d], part_recv.at[d], d) for d in range(1, n_tp)]
    for copy in parts:
        copy.start()
    own = jnp.dot(head_mix, wo_ref[:, columns(0)], preferred_element_type=f32)
    attn = rounded(own)
    token_block = tokens_ref[:, columns(0)].astype(f32)
    for copy in parts:
        copy.wait_recv()
    for d in range(1, n_tp):
        attn = attn + part_in[d].astype(f32)
    residual = (token_block + attn).astype(bf16)
    gathered[col, me] = residual

    rings = [to_ep(gathered.at[col, me], gathered.at[col, me], ring_send.at[k], ring_recv.at[me], peers[k]) for k in far_first]
    for copy in rings:
        copy.start()
    fans = []
    if n_tp == 4:
        beside = col + 1 - 2 * lax.rem(col, 2)
        across = lax.rem(col + 2, 4)
        routes, first = ((col, across), (col, beside), (across, beside)), 2
    else:
        routes, first = tuple((col, lax.rem(col + d, n_tp)) for d in range(1, n_tp)), n_tp - 1

    def fan_copies(k, slot):
        return [
            pltpu.make_async_remote_copy(
                src_ref=gathered.at[block, slot], dst_ref=gathered.at[block, slot],
                send_sem=fan_send.at[k, d], recv_sem=fan_recv.at[k, d],
                device_id={"tp": target}, device_id_type=MESH)
            for d, (block, target) in enumerate(routes)
        ]

    def arrive(k):
        slot = peers[k]
        if k > 0:
            to_ep(gathered.at[col, slot], gathered.at[col, slot], ring_send.at[k], ring_recv.at[slot], slot).wait_recv()
        fan = fan_copies(k, slot)
        for copy in fan[:first]:
            copy.start()
        fans.append(fan)

    arrive(0)
    for load in later[1:5]:
        load.wait()
    expert = me
    hit = jnp.zeros((1, batch), f32)
    weight_row = jnp.zeros((1, batch), f32)
    for k in range(ids_ref.shape[0]):
        same = ids_ref[k:k + 1, :] == expert
        hit = hit + jnp.where(same, 1.0, 0.0)
        weight_row = weight_row + jnp.where(same, route_ref[k:k + 1, :], 0.0)
    row_at = iota((batch, batch), 0)
    col_at = iota((batch, batch), 1)
    before = (row_at <= col_at) & (row_at >= group_of(col_at, seq_rows) * seq_rows)
    hits = jnp.broadcast_to(hit, (8, batch))
    rank = jnp.dot(hits.astype(bf16), before.astype(f32).astype(bf16), preferred_element_type=f32)[0:1]
    slot_of = jnp.where((hit > 0.5) & (rank < cap + 0.5), group_of(iota((1, batch), 1), seq_rows) * cap + rank - 1.0, -1.0)
    pick_f = jnp.where(iota((slots, batch), 0) == slot_of, 1.0, 0.0)
    pick = pick_f.astype(bf16)
    place = pick_f.T.astype(bf16)
    weight = jnp.sum((pick_f * weight_row).T, axis=1, keepdims=True)
    for k in range(1, n_ep):
        arrive(k)

    for k in range(n_ep + 1):
        if k < n_ep and first < len(routes):
            fans[k][0].wait_recv()
            fans[k][2].start()
        k = k - 1
        if k < 0:
            continue
        for copy in (fans[k][1:] if first < len(routes) else fans[k]):
            copy.wait_recv()
        slot = peers[k]
        blocks = [gathered[t, slot].astype(f32) for t in range(n_tp)]
        squares = sum(jnp.sum(b * b, axis=1, keepdims=True) for b in blocks)
        scale = lax.rsqrt(squares / width + EPSILON)
        for t in range(n_tp):
            rows_f[pl.ds(pl.multiple_of(slot * seq_rows, 8), seq_rows), t * span:(t + 1) * span] = (
                blocks[t] * scale * gain_ref[:, t * span:(t + 1) * span])
    normed = rows_f[...].astype(bf16)

    picked = jnp.dot(pick, normed, preferred_element_type=f32).astype(bf16)
    for load in later[5:8]:
        load.wait()
    gate = jnp.dot(picked, wg[...], preferred_element_type=f32)
    up = jnp.dot(picked, wu[...], preferred_element_type=f32)
    hidden = (gate / (1.0 + jnp.exp(-gate)) * up).astype(bf16)
    moves = []
    for d in sorted(range(1, n_tp), key=lambda d: d != 2):
        exp_out[d] = jnp.dot(hidden, wd[:, columns(d)], preferred_element_type=f32).astype(bf16)
        copy = to_tp(exp_out.at[d], exp_in.at[d], exp_send.at[d], exp_recv.at[d], d)
        copy.start()
        moves.append(copy)
    expert_rows = rounded(jnp.dot(hidden, wd[:, columns(0)], preferred_element_type=f32))

    shared_tiles = shared_ref[...].astype(f32)
    shared = jnp.concatenate([shared_tiles[i:i + 1] for i in range(width // 128)], axis=1)
    for load in later[8:]:
        load.wait()
    step = seq_rows * 8 if n_ep % 8 == 0 else batch

    def dense(at):
        rows = rows_f[pl.ds(at, step), :].astype(bf16)
        gate = lax.dot_general(rows, dg[...], contract, preferred_element_type=f32)
        up = lax.dot_general(rows, du[...], contract, preferred_element_type=f32)
        hidden = (gate / (1.0 + jnp.exp(-gate)) * up).astype(bf16)
        mix = jnp.sum(rows.astype(f32) * shared, axis=1, keepdims=True)
        mix = 1.0 / (1.0 + jnp.exp(-mix))
        total[pl.ds(at, step), :] = mix * jnp.dot(hidden, dd[...], preferred_element_type=f32)

    if step == batch:
        dense(0)
    else:
        @pl.loop(0, batch // step)
        def _(i):
            dense(pl.multiple_of(i * step, step))

    for copy in moves:
        copy.wait_recv()
    for d in range(1, n_tp):
        expert_rows = expert_rows + exp_in[d].astype(f32)
    placed = jnp.dot(place, expert_rows.astype(bf16), preferred_element_type=f32)
    total[...] = total[...] + placed * weight

    sums = []
    for k in far_first:
        slot = peers[k]
        sum_out[k] = total[pl.ds(pl.multiple_of(slot * seq_rows, 8), seq_rows), :].astype(bf16)
        copy = to_ep(sum_out.at[k], sum_in.at[me], sum_send.at[k], sum_recv.at[me], slot)
        copy.start()
        sums.append(copy)
    result = residual.astype(f32) + total[pl.ds(pl.multiple_of(me * seq_rows, 8), seq_rows), :]
    for k in range(1, n_ep):
        slot = peers[k]
        to_ep(sum_out.at[k], sum_in.at[slot], sum_send.at[k], sum_recv.at[slot], slot).wait_recv()
        result = result + sum_in[slot].astype(f32)
    out_ref[...] = result.astype(bf16)
    for copy in parts + rings + [c for fan in fans for c in fan] + moves + sums:
        copy.wait_send()


def layer_call(tokens, attn_gain, w_query, w_key, w_value, w_forget, forget_bias, query_gain, key_gain,
              cache_pairs, cache_cum, lengths, w_output, ffn_gain, expert_ids, route_weight, shared_gate,
              w_exp_gate, w_exp_up, w_exp_down, w_dense_gate, w_dense_up, w_dense_down):
    n_ep, n_tp = lax.axis_size("ep"), lax.axis_size("tp")
    seq_rows, width = tokens.shape
    cap = max(2, min(seq_rows, 128 // n_ep))
    span = width // n_tp
    slots, batch = n_ep * cap, n_ep * seq_rows
    bf16, f32 = jnp.bfloat16, jnp.float32
    vmem = pl.BlockSpec(memory_space=pltpu.VMEM)
    hbm = pl.BlockSpec(memory_space=pltpu.HBM)
    dma = pltpu.SemaphoreType.DMA
    return pl.pallas_call(
        functools.partial(whole_layer, n_ep, n_tp, cap),
        out_shape=pltpu.VMEM((seq_rows, span), bf16),
        in_specs=[hbm] * 23,
        out_specs=vmem,
        scratch_shapes=[
            pltpu.VMEM(tokens.shape, bf16),
            pltpu.VMEM((1, width), f32),
            pltpu.VMEM((1, query_gain.shape[0]), f32),
            pltpu.VMEM((1, key_gain.shape[0]), f32),
            pltpu.VMEM((1, width), bf16),
            pltpu.VMEM((1, 1), f32),
            pltpu.VMEM((1, seq_rows), jnp.int32),
            pltpu.VMEM((1, width), f32),
            pltpu.VMEM(expert_ids.shape[::-1], jnp.int32),
            pltpu.VMEM(route_weight.shape[::-1], f32),
            pltpu.VMEM((width // 128, 128), bf16),
            pltpu.VMEM(w_query.shape, bf16),
            pltpu.VMEM((2 * w_key.shape[1], width), bf16),
            pltpu.VMEM((seq_rows, cache_cum.shape[2]), f32),
            pltpu.VMEM((seq_rows,) + cache_pairs.shape[2:], bf16),
            pltpu.VMEM(w_output.shape, bf16),
            pltpu.VMEM((seq_rows, w_query.shape[1]), f32),
            pltpu.VMEM(w_exp_gate.shape[1:], bf16),
            pltpu.VMEM(w_exp_up.shape[1:], bf16),
            pltpu.VMEM(w_exp_down.shape[1:], bf16),
            pltpu.VMEM(w_dense_gate.shape, bf16),
            pltpu.VMEM(w_dense_up.shape, bf16),
            pltpu.VMEM(w_dense_down.shape, bf16),
            pltpu.VMEM((n_tp, seq_rows, span), bf16),
            pltpu.VMEM((n_tp, seq_rows, span), bf16),
            pltpu.VMEM((n_tp, n_ep, seq_rows, span), bf16),
            pltpu.VMEM((batch, width), f32),
            pltpu.VMEM((n_tp, slots, span), bf16),
            pltpu.VMEM((n_tp, slots, span), bf16),
            pltpu.VMEM((batch, span), f32),
            pltpu.VMEM((n_ep, seq_rows, span), bf16),
            pltpu.VMEM((n_ep, seq_rows, span), bf16),
            dma((11,)),
            dma((seq_rows // 4,)),
            dma((11,)),
            dma((n_tp,)), dma((n_tp,)),
            dma((n_ep,)), dma((n_ep,)),
            dma((n_ep, n_tp)), dma((n_ep, n_tp)),
            dma((n_tp,)), dma((n_tp,)),
            dma((n_ep,)), dma((n_ep,)),
        ],
        compiler_params=pltpu.CompilerParams(
            collective_id=0, has_side_effects=True, vmem_limit_bytes=VMEM_BYTES),
        name="whole_layer",
    )(tokens, attn_gain.reshape(1, width), query_gain.reshape(1, -1), key_gain.reshape(1, -1),
      w_forget.reshape(1, width), forget_bias.reshape(1, 1), lengths.reshape(1, seq_rows),
      ffn_gain.reshape(1, width), expert_ids.T, route_weight.T, shared_gate.reshape(width // 128, 128),
      w_query, w_key.T, w_value.T, cache_cum, cache_pairs, w_output,
      w_exp_gate, w_exp_up, w_exp_down,
      w_dense_gate, w_dense_up, w_dense_down)


def shards(
    tokens,
    attn_gain,
    w_query,
    w_key,
    w_value,
    w_forget,
    forget_bias,
    query_gain,
    key_gain,
    cache_pairs,
    cache_cum,
    lengths,
    w_output,
    ffn_gain,
    expert_ids,
    route_weight,
    w_exp_gate,
    w_exp_up,
    w_exp_down,
    shared_gate,
    w_dense_gate,
    w_dense_up,
    w_dense_down,
):
    return layer_call(
        tokens, attn_gain, w_query, w_key, w_value, w_forget, forget_bias, query_gain, key_gain,
        cache_pairs, cache_cum, lengths, w_output, ffn_gain, expert_ids, route_weight, shared_gate,
        w_exp_gate, w_exp_up, w_exp_down, w_dense_gate, w_dense_up, w_dense_down,
    )


def solution(mesh):
    in_specs = (
        P("ep", None),
        P(),
        P(None, "tp"),
        P(None, "tp"),
        P(None, "tp"),
        P(None, "tp"),
        P("tp"),
        P(),
        P(),
        P("ep", "tp", None, None),
        P("ep", "tp", None),
        P("ep"),
        P("tp", None),
        P(),
        P(),
        P(),
        P("ep", None, "tp"),
        P("ep", None, "tp"),
        P("ep", "tp", None),
        P(),
        P("ep", None),
        P("ep", None),
        P("ep", "tp"),
    )
    out_specs = P("ep", "tp")
    return jax.shard_map(shards, mesh=mesh, in_specs=in_specs, out_specs=out_specs, check_vma=False)
```

time: 38.9 us -> 34.8 us (0.89)
  Pallas kernels: 36.7 us -> 33.4 us
  local copies, waits for them, and re-layouts: 1.31 us -> 0.6 us
    pallas_call x1, Pallas kernels: 36.7 us -> 33.4 us  [layer_call(): pl.pallas_call(functools.partial(whole_layer, n_ep, n_tp, cap), out_shape...]
    unnamed x1, local copies, waits for them, and re-layouts: 1.31 us -> 0.6 us
where the time goes in v1:
time: 34.8 us; the launch traced here: 34.7 us
  Pallas kernels  33.4 us (96%)
  between operations  0.66 us (2%)
  local copies, waits for them, and re-layouts  0.6 us (2%)
    pallas_call x1, Pallas kernels, layer_call(): pl.pallas_call(functools.partial(whole_layer, n_ep, n_tp, cap), out_shape...  33.4 us

profile of v1, /device:TPU:0, one launch (start us, length us, event | category | flops | bytes accessed | tf_op | source)
XLA Modules:
  0.0 34.7 jit_solution(2855196813770750544)
XLA Ops:
  0.7 33.4 %whole_layer.1 = bf16[24,256]{1,0:T(8,128)(2,1)S(1)} custom-call(bf16[24,1024]{1,0:T(8,128)(2,1)} %tokens_hbm.1, f32[1,1024]{1,0:T(1,128)} %bitcast.15, f32[1,64]{1,0:T(1,128)} %bitcast.21, f32[1,64]{1,0:T(1,128)} %bitcast.22, bf16[1,1024]{1,0:T(2,128)(2,1)} %bitcast.16, f32[1,1]{1,0:T(1,128)} %bitcast.12.bias_hbm, s32[1,24]{1,0:T(1,128)} %bitcast.23, ...), custom_call_target="tpu_custom_call" | custom-call | tf_op jit(solution)/shard_map/whole_layer/pallas_call | solution.py:358
  34.1 0.6 %copy.25 = bf16[24,256]{1,0:T(8,128)(2,1)} copy(bf16[24,256]{1,0:T(8,128)(2,1)S(1)} %whole_layer.1) | data formatting | bytes 24576

commit v2 on v1

--- a/solution.py
+++ b/solution.py
@@ -23,8 +23,8 @@
     gain_ref, ids_ref, route_ref, shared_ref,
     wq, wkv, cum, cache, wo_ref, mixed,
     wg, wu, wd, dg, du, dd,
-    part_out, part_in, gathered, rows_f, exp_out, exp_in, total, sum_out, sum_in,
-    small_sem, attn_sem, load_sem, part_send, part_recv, ring_send, ring_recv, fan_send, fan_recv,
+    part_out, part_in, gathered, rows_f, pick_ref, place_ref, weight_ref, exp_out, exp_in, total, sum_out, sum_in,
+    small_sem, attn_sem, load_sem, part_send, part_recv, ring_send, ring_recv, fan_send, fan_recv, cross_recv,
     exp_send, exp_recv, sum_send, sum_recv,
 ):
     me = lax.axis_index("ep")
@@ -38,7 +38,7 @@
     heads = wq.shape[1] // head
     lanes = 2 * head
     eight = 8
-    bunch = 4
+    bunch = eight
     small = [
         pltpu.make_async_copy(src, dst, small_sem.at[i])
         for i, (src, dst) in enumerate((
@@ -89,6 +89,7 @@
         peers = [line[k // 2] * 2 + (side if k % 2 == 0 else 1 - side) for k in range(n_ep)]
     else:
         peers = [lax.rem(me + k, n_ep) for k in range(n_ep)]
+    sets = [list(range(4)), list(range(4, 8))] if n_ep == 8 else [list(range(n_ep))]
     far_first = list(range(n_ep - 1, 0, -1))
 
     contract = (((1,), (1,)), ((), ()))
@@ -197,50 +198,60 @@
     head_mix = mixed[...].astype(bf16)
     later[0].wait()
 
+    partial = jnp.dot(head_mix, wo_ref[...], preferred_element_type=f32).astype(bf16)
+    for j in range(n_tp):
+        part_out[j] = partial[:, j * span:(j + 1) * span]
+    pl.semaphore_wait(barrier, n_ep + n_tp - 2)
     for d in range(1, n_tp):
-        part_out[d] = jnp.dot(head_mix, wo_ref[:, columns(d)], preferred_element_type=f32).astype(bf16)
-    pl.semaphore_wait(barrier, n_ep + n_tp - 2)
-    parts = [to_tp(part_out.at[d], part_in.at[d], part_send.at[d], part_recv.at[d], d) for d in range(1, n_tp)]
-    for copy in parts:
-        copy.start()
-    own = jnp.dot(head_mix, wo_ref[:, columns(0)], preferred_element_type=f32)
-    attn = rounded(own)
+        there = lax.rem(col + d, n_tp)
+        to_tp(part_out.at[there], part_in.at[col], part_send, part_recv, d).start()
+    some = pl.ds(0, n_tp - 1)
+    parts = to_tp(part_out.at[some], part_in.at[some], part_send, part_recv, 1)
     token_block = tokens_ref[:, columns(0)].astype(f32)
-    for copy in parts:
-        copy.wait_recv()
-    for d in range(1, n_tp):
-        attn = attn + part_in[d].astype(f32)
+    part_in[col] = part_out[col]
+    parts.wait_recv()
+    attn = part_in[0].astype(f32)
+    for j in range(1, n_tp):
+        attn = attn + part_in[j].astype(f32)
     residual = (token_block + attn).astype(bf16)
     gathered[col, me] = residual
 
-    rings = [to_ep(gathered.at[col, me], gathered.at[col, me], ring_send.at[k], ring_recv.at[me], peers[k]) for k in far_first]
-    for copy in rings:
-        copy.start()
-    fans = []
+    for k in far_first:
+        to_ep(gathered.at[col, me], gathered.at[col, me], ring_send, ring_recv.at[me], peers[k]).start()
     if n_tp == 4:
-        beside = col + 1 - 2 * lax.rem(col, 2)
-        across = lax.rem(col + 2, 4)
-        routes, first = ((col, across), (col, beside), (across, beside)), 2
+        across, beside = lax.rem(col + 2, 4), col + 1 - 2 * lax.rem(col, 2)
+        others = [across, lax.rem(col + 2, 4) + 1 - 2 * lax.rem(col, 2), beside]
+        relayed = [k for k in range(n_ep) if k < 0]
     else:
-        routes, first = tuple((col, lax.rem(col + d, n_tp)) for d in range(1, n_tp)), n_tp - 1
-
-    def fan_copies(k, slot):
-        return [
-            pltpu.make_async_remote_copy(
-                src_ref=gathered.at[block, slot], dst_ref=gathered.at[block, slot],
-                send_sem=fan_send.at[k, d], recv_sem=fan_recv.at[k, d],
-                device_id={"tp": target}, device_id_type=MESH)
-            for d, (block, target) in enumerate(routes)
-        ]
+        across, beside = col, col
+        others = [lax.rem(col + d, n_tp) for d in range(1, n_tp)]
+        relayed = []
+
+    def to_other(block, slot, recv, other):
+        return pltpu.make_async_remote_copy(
+            src_ref=gathered.at[block, slot], dst_ref=gathered.at[block, slot],
+            send_sem=fan_send, recv_sem=recv, device_id={"tp": other}, device_id_type=MESH)
 
     def arrive(k):
         slot = peers[k]
         if k > 0:
-            to_ep(gathered.at[col, slot], gathered.at[col, slot], ring_send.at[k], ring_recv.at[slot], slot).wait_recv()
-        fan = fan_copies(k, slot)
-        for copy in fan[:first]:
-            copy.start()
-        fans.append(fan)
+            to_ep(gathered.at[col, slot], gathered.at[col, slot], ring_send, ring_recv.at[slot], slot).wait_recv()
+        if k in relayed:
+            to_other(col, slot, cross_recv.at[k], across).start()
+            to_other(col, slot, fan_recv.at[k], beside).start()
+        else:
+            for other in others:
+                to_other(col, slot, fan_recv.at[k], other).start()
+
+    def relay(k):
+        to_other(col, peers[k], cross_recv.at[k], across).wait_recv()
+        to_other(across, peers[k], fan_recv.at[k], beside).start()
+
+    def spread(k, blocks):
+        group = gathered.at[pl.ds(0, blocks), peers[k]]
+        return pltpu.make_async_remote_copy(
+            src_ref=group, dst_ref=group, send_sem=fan_send, recv_sem=fan_recv.at[k],
+            device_id={"tp": others[0]}, device_id_type=MESH)
 
     arrive(0)
     for load in later[1:5]:
@@ -254,93 +265,126 @@
         weight_row = weight_row + jnp.where(same, route_ref[k:k + 1, :], 0.0)
     row_at = iota((batch, batch), 0)
     col_at = iota((batch, batch), 1)
+    hits = jnp.broadcast_to(hit, (8, batch)).astype(bf16)
+    if len(sets) > 1:
+        lane = iota((1, batch), 1)
+        block = group_of(lane, seq_rows)
+        source = lane - block * seq_rows
+        for k in range(n_ep):
+            source = source + jnp.where(block == k, (peers[k] * seq_rows).astype(f32), 0.0)
+        turn = jnp.where(row_at == source, 1.0, 0.0)
+        hits = jnp.dot(hits, turn.astype(bf16), preferred_element_type=f32).astype(bf16)
+        weight_row = jnp.dot(
+            jnp.broadcast_to(weight_row, (8, batch)), turn,
+            precision=lax.Precision.HIGHEST, preferred_element_type=f32)[0:1]
+    hit = hits[0:1].astype(f32)
     before = (row_at <= col_at) & (row_at >= group_of(col_at, seq_rows) * seq_rows)
-    hits = jnp.broadcast_to(hit, (8, batch))
-    rank = jnp.dot(hits.astype(bf16), before.astype(f32).astype(bf16), preferred_element_type=f32)[0:1]
+    rank = jnp.dot(hits, before.astype(f32).astype(bf16), preferred_element_type=f32)[0:1]
     slot_of = jnp.where((hit > 0.5) & (rank < cap + 0.5), group_of(iota((1, batch), 1), seq_rows) * cap + rank - 1.0, -1.0)
-    pick_f = jnp.where(iota((slots, batch), 0) == slot_of, 1.0, 0.0)
-    pick = pick_f.astype(bf16)
-    place = pick_f.T.astype(bf16)
-    weight = jnp.sum((pick_f * weight_row).T, axis=1, keepdims=True)
-    for k in range(1, n_ep):
-        arrive(k)
-
-    for k in range(n_ep + 1):
-        if k < n_ep and first < len(routes):
-            fans[k][0].wait_recv()
-            fans[k][2].start()
-        k = k - 1
-        if k < 0:
-            continue
-        for copy in (fans[k][1:] if first < len(routes) else fans[k]):
-            copy.wait_recv()
-        slot = peers[k]
-        blocks = [gathered[t, slot].astype(f32) for t in range(n_tp)]
+    for n, chosen in enumerate(sets):
+        lines = len(chosen) * seq_rows
+        places = len(chosen) * cap
+        here = slot_of[:, n * lines:(n + 1) * lines]
+        pick = jnp.where(iota((places, lines), 0) + n * places == here, 1.0, 0.0)
+        pick_ref[n] = pick.astype(bf16)
+        place_ref[n] = pick.T.astype(bf16)
+        weight_ref[n] = jnp.sum((pick * weight_row[:, n * lines:(n + 1) * lines]).T, axis=1, keepdims=True)
+    shared_tiles = shared_ref[...].astype(f32)
+    shared = jnp.concatenate([shared_tiles[i:i + 1] for i in range(width // 128)], axis=1)
+
+    def lines_of(k):
+        at = k * seq_rows if len(sets) > 1 else pl.multiple_of(peers[k] * seq_rows, 8)
+        return pl.ds(at, seq_rows)
+
+    def normalize(k):
+        blocks = [gathered[t, peers[k]].astype(f32) for t in range(n_tp)]
         squares = sum(jnp.sum(b * b, axis=1, keepdims=True) for b in blocks)
         scale = lax.rsqrt(squares / width + EPSILON)
         for t in range(n_tp):
-            rows_f[pl.ds(pl.multiple_of(slot * seq_rows, 8), seq_rows), t * span:(t + 1) * span] = (
+            rows_f[lines_of(k), t * span:(t + 1) * span] = (
                 blocks[t] * scale * gain_ref[:, t * span:(t + 1) * span])
-    normed = rows_f[...].astype(bf16)
-
-    picked = jnp.dot(pick, normed, preferred_element_type=f32).astype(bf16)
-    for load in later[5:8]:
-        load.wait()
-    gate = jnp.dot(picked, wg[...], preferred_element_type=f32)
-    up = jnp.dot(picked, wu[...], preferred_element_type=f32)
-    hidden = (gate / (1.0 + jnp.exp(-gate)) * up).astype(bf16)
-    moves = []
-    for d in sorted(range(1, n_tp), key=lambda d: d != 2):
-        exp_out[d] = jnp.dot(hidden, wd[:, columns(d)], preferred_element_type=f32).astype(bf16)
-        copy = to_tp(exp_out.at[d], exp_in.at[d], exp_send.at[d], exp_recv.at[d], d)
-        copy.start()
-        moves.append(copy)
-    expert_rows = rounded(jnp.dot(hidden, wd[:, columns(0)], preferred_element_type=f32))
-
-    shared_tiles = shared_ref[...].astype(f32)
-    shared = jnp.concatenate([shared_tiles[i:i + 1] for i in range(width // 128)], axis=1)
-    for load in later[8:]:
-        load.wait()
-    step = seq_rows * 8 if n_ep % 8 == 0 else batch
-
-    def dense(at):
-        rows = rows_f[pl.ds(at, step), :].astype(bf16)
+
+    def expert_part(n, chosen):
+        lines = len(chosen) * seq_rows
+        rows = rows_f[n * lines:(n + 1) * lines, :].astype(bf16)
+        picked = jnp.dot(pick_ref[n], rows, preferred_element_type=f32).astype(bf16)
+        gate = jnp.dot(picked, wg[...], preferred_element_type=f32)
+        up = jnp.dot(picked, wu[...], preferred_element_type=f32)
+        hidden = (gate / (1.0 + jnp.exp(-gate)) * up).astype(bf16)
+        down = jnp.dot(hidden, wd[...], preferred_element_type=f32).astype(bf16)
+        for j in range(n_tp):
+            exp_out[n, j] = down[:, j * span:(j + 1) * span]
+        for d in sorted(range(1, n_tp), key=lambda d: d != 2):
+            there = lax.rem(col + d, n_tp)
+            to_tp(exp_out.at[n, there], exp_in.at[n, col], exp_send.at[n], exp_recv.at[n], d).start()
+        exp_in[n, col] = exp_out[n, col]
+
+    def moves(n):
+        there = pl.ds(0, n_tp - 1)
+        return to_tp(exp_out.at[n, there], exp_in.at[n, there], exp_send.at[n], exp_recv.at[n], 1)
+
+    def dense(rows):
+        rows = rows.astype(bf16)
         gate = lax.dot_general(rows, dg[...], contract, preferred_element_type=f32)
         up = lax.dot_general(rows, du[...], contract, preferred_element_type=f32)
         hidden = (gate / (1.0 + jnp.exp(-gate)) * up).astype(bf16)
         mix = jnp.sum(rows.astype(f32) * shared, axis=1, keepdims=True)
         mix = 1.0 / (1.0 + jnp.exp(-mix))
-        total[pl.ds(at, step), :] = mix * jnp.dot(hidden, dd[...], preferred_element_type=f32)
-
+        return mix * jnp.dot(hidden, dd[...], preferred_element_type=f32)
+
+    def finish(n, chosen):
+        moves(n).wait_recv()
+        rows = exp_in[n, 0].astype(f32)
+        for j in range(1, n_tp):
+            rows = rows + exp_in[n, j].astype(f32)
+        placed = jnp.dot(place_ref[n], rows.astype(bf16), preferred_element_type=f32) * weight_ref[n]
+        lines = len(chosen) * seq_rows
+        total[n * lines:(n + 1) * lines, :] = total[n * lines:(n + 1) * lines, :] + placed
+        for k in reversed(chosen):
+            if k > 0:
+                sum_out[k] = total[lines_of(k), :].astype(bf16)
+        for k in reversed(chosen):
+            if k > 0:
+                to_ep(sum_out.at[k], sum_in.at[me], sum_send, sum_recv.at[me], peers[k]).start()
+
+    for k in range(1, n_ep):
+        arrive(k)
+        if k - 4 in relayed:
+            relay(k - 4)
+    for load in later[5:]:
+        load.wait()
+    for n, chosen in enumerate(sets):
+        for k in chosen:
+            if k > n_ep - 1 - 4 and k in relayed:
+                relay(k)
+            spread(k, 2 if k in relayed else n_tp - 1).wait_recv()
+        for k in chosen:
+            normalize(k)
+        expert_part(n, chosen)
+    step = seq_rows * 8 if n_ep % 8 == 0 else batch
     if step == batch:
-        dense(0)
+        total[...] = dense(rows_f[...])
     else:
         @pl.loop(0, batch // step)
         def _(i):
-            dense(pl.multiple_of(i * step, step))
-
-    for copy in moves:
-        copy.wait_recv()
-    for d in range(1, n_tp):
-        expert_rows = expert_rows + exp_in[d].astype(f32)
-    placed = jnp.dot(place, expert_rows.astype(bf16), preferred_element_type=f32)
-    total[...] = total[...] + placed * weight
-
-    sums = []
-    for k in far_first:
-        slot = peers[k]
-        sum_out[k] = total[pl.ds(pl.multiple_of(slot * seq_rows, 8), seq_rows), :].astype(bf16)
-        copy = to_ep(sum_out.at[k], sum_in.at[me], sum_send.at[k], sum_recv.at[me], slot)
-        copy.start()
-        sums.append(copy)
-    result = residual.astype(f32) + total[pl.ds(pl.multiple_of(me * seq_rows, 8), seq_rows), :]
+            at = pl.multiple_of(i * step, step)
+            total[pl.ds(at, step), :] = dense(rows_f[pl.ds(at, step), :])
+    for n, chosen in enumerate(sets):
+        finish(n, chosen)
+    result = residual.astype(f32) + total[lines_of(0), :]
     for k in range(1, n_ep):
         slot = peers[k]
-        to_ep(sum_out.at[k], sum_in.at[slot], sum_send.at[k], sum_recv.at[slot], slot).wait_recv()
+        to_ep(sum_out.at[k], sum_in.at[slot], sum_send, sum_recv.at[slot], slot).wait_recv()
         result = result + sum_in[slot].astype(f32)
     out_ref[...] = result.astype(bf16)
-    for copy in parts + rings + [c for fan in fans for c in fan] + moves + sums:
-        copy.wait_send()
+    parts.wait_send()
+    others_of = gathered.at[0, pl.ds(0, n_ep - 1)]
+    to_ep(others_of, others_of, ring_send, ring_recv.at[0], peers[1]).wait_send()
+    for k in range(n_ep):
+        spread(k, n_tp - 1).wait_send()
+    for n in range(len(sets)):
+        moves(n).wait_send()
+    to_ep(sum_out.at[pl.ds(1, n_ep - 1)], sum_in.at[pl.ds(1, n_ep - 1)], sum_send, sum_recv.at[1], peers[1]).wait_send()
 
 
 def layer_call(tokens, attn_gain, w_query, w_key, w_value, w_forget, forget_bias, query_gain, key_gain,
@@ -349,6 +393,7 @@
     n_ep, n_tp = lax.axis_size("ep"), lax.axis_size("tp")
     seq_rows, width = tokens.shape
     cap = max(2, min(seq_rows, 128 // n_ep))
+    n_sets = 2 if n_ep == 8 else 1
     span = width // n_tp
     slots, batch = n_ep * cap, n_ep * seq_rows
     bf16, f32 = jnp.bfloat16, jnp.float32
@@ -388,19 +433,22 @@
             pltpu.VMEM((n_tp, seq_rows, span), bf16),
             pltpu.VMEM((n_tp, n_ep, seq_rows, span), bf16),
             pltpu.VMEM((batch, width), f32),
-            pltpu.VMEM((n_tp, slots, span), bf16),
-            pltpu.VMEM((n_tp, slots, span), bf16),
+            pltpu.VMEM((n_sets, slots // n_sets, batch // n_sets), bf16),
+            pltpu.VMEM((n_sets, batch // n_sets, slots // n_sets), bf16),
+            pltpu.VMEM((n_sets, batch // n_sets, 1), f32),
+            pltpu.VMEM((n_sets, n_tp, slots // n_sets, span), bf16),
+            pltpu.VMEM((n_sets, n_tp, slots // n_sets, span), bf16),
             pltpu.VMEM((batch, span), f32),
             pltpu.VMEM((n_ep, seq_rows, span), bf16),
             pltpu.VMEM((n_ep, seq_rows, span), bf16),
             dma((11,)),
-            dma((seq_rows // 4,)),
+            dma((seq_rows // 8,)),
             dma((11,)),
-            dma((n_tp,)), dma((n_tp,)),
-            dma((n_ep,)), dma((n_ep,)),
-            dma((n_ep, n_tp)), dma((n_ep, n_tp)),
-            dma((n_tp,)), dma((n_tp,)),
-            dma((n_ep,)), dma((n_ep,)),
+            dma, dma,
+            dma, dma((n_ep,)),
+            dma, dma((n_ep,)), dma((n_ep,)),
+            dma((n_sets,)), dma((n_sets,)),
+            dma, dma((n_ep,)),
         ],
         compiler_params=pltpu.CompilerParams(
             collective_id=0, has_side_effects=True, vmem_limit_bytes=VMEM_BYTES),

time: 34.8 us -> 32 us (0.920)
  Pallas kernels: 33.4 us -> 30.6 us
    pallas_call x1, Pallas kernels: 33.4 us -> 30.6 us  [layer_call(): pl.pallas_call(functools.partial(whole_layer, n_ep, n_tp, cap), out_shape...]
where the time goes in v2:
time: 32 us; the launch traced here: 31.9 us
  Pallas kernels  30.6 us (96%)
  between operations  0.66 us (2%)
  local copies, waits for them, and re-layouts  0.6 us (2%)
    pallas_call x1, Pallas kernels, layer_call(): pl.pallas_call(functools.partial(whole_layer, n_ep, n_tp, cap), out_shape...  30.6 us

profile of v2, /device:TPU:0, one launch (start us, length us, event | category | flops | bytes accessed | tf_op | source)
XLA Modules:
  0.0 31.9 jit_solution(9686021995557224604)
XLA Ops:
  0.7 30.6 %whole_layer.1 = bf16[24,256]{1,0:T(8,128)(2,1)S(1)} custom-call(bf16[24,1024]{1,0:T(8,128)(2,1)} %tokens_hbm.1, f32[1,1024]{1,0:T(1,128)} %bitcast.15, f32[1,64]{1,0:T(1,128)} %bitcast.21, f32[1,64]{1,0:T(1,128)} %bitcast.22, bf16[1,1024]{1,0:T(2,128)(2,1)} %bitcast.16, f32[1,1]{1,0:T(1,128)} %bitcast.12.bias_hbm, s32[1,24]{1,0:T(1,128)} %bitcast.23, ...), custom_call_target="tpu_custom_call" | custom-call | tf_op jit(solution)/shard_map/whole_layer/pallas_call | solution.py:403
  31.3 0.6 %copy.25 = bf16[24,256]{1,0:T(8,128)(2,1)} copy(bf16[24,256]{1,0:T(8,128)(2,1)S(1)} %whole_layer.1) | data formatting | bytes 24576

commit v3 on v2

--- a/solution.py
+++ b/solution.py
@@ -10,6 +10,12 @@
 EPSILON = 1e-06
 MESH = pl.DeviceIdType.MESH
 VMEM_BYTES = 56 * 1024 * 1024
+
+
+def block_sets(n_ep):
+    if n_ep == 8:
+        return [[0, 1], [2, 3], [4, 5, 6, 7]]
+    return [list(range(n_ep))]
 
 
 def whole_layer(
@@ -22,9 +28,9 @@
     tokens_ref, attn_gain_ref, query_gain_ref, key_gain_ref, forget_ref, bias_ref, length_ref,
     gain_ref, ids_ref, route_ref, shared_ref,
     wq, wkv, cum, cache, wo_ref, mixed,
-    wg, wu, wd, dg, du, dd,
+    wgu, wd, dgu, dd,
     part_out, part_in, gathered, rows_f, pick_ref, place_ref, weight_ref, exp_out, exp_in, total, sum_out, sum_in,
-    small_sem, attn_sem, load_sem, part_send, part_recv, ring_send, ring_recv, fan_send, fan_recv, cross_recv,
+    small_sem, attn_sem, load_sem, part_send, part_recv, ring_send, ring_recv, fan_send, fan_recv,
     exp_send, exp_recv, sum_send, sum_recv,
 ):
     me = lax.axis_index("ep")
@@ -43,10 +49,12 @@
         pltpu.make_async_copy(src, dst, small_sem.at[i])
         for i, (src, dst) in enumerate((
             (tokens_hbm, tokens_ref), (attn_gain_hbm, attn_gain_ref), (wq_hbm, wq),
-            (wk_hbm, wkv.at[pl.ds(0, head)]), (wv_hbm, wkv.at[pl.ds(head, head)]),
+            (wk_hbm, wkv.at[pl.ds(0, head)]),
             (forget_hbm, forget_ref), (bias_hbm, bias_ref), (length_hbm, length_ref),
             (query_gain_hbm, query_gain_ref), (key_gain_hbm, key_gain_ref), (cum_hbm.at[:, 0], cum)))
     ]
+    small.insert(4, pltpu.make_async_copy(wv_hbm, wkv.at[pl.ds(head, head)], small_sem.at[3]))
+    both = pltpu.make_async_copy(wkv, wkv, small_sem.at[3])
     caches = [
         pltpu.make_async_copy(cache_hbm.at[pl.ds(b, bunch), 0], cache.at[pl.ds(b, bunch)], attn_sem.at[b // bunch])
         for b in range(0, seq_rows, bunch)
@@ -55,9 +63,12 @@
         pltpu.make_async_copy(src, dst, load_sem.at[i])
         for i, (src, dst) in enumerate((
             (wo_hbm, wo_ref), (gain_hbm, gain_ref), (ids_hbm, ids_ref), (route_hbm, route_ref),
-            (shared_hbm, shared_ref), (wg_hbm.at[0], wg), (wu_hbm.at[0], wu), (wd_hbm.at[0], wd),
-            (dg_hbm, dg), (du_hbm, du), (dd_hbm, dd)))
+            (shared_hbm, shared_ref), (wg_hbm, wgu.at[pl.ds(0, 1)]), (wd_hbm.at[0], wd),
+            (dg_hbm, dgu.at[0]), (dd_hbm, dd)))
     ]
+    later.insert(6, pltpu.make_async_copy(wu_hbm, wgu.at[pl.ds(1, 1)], load_sem.at[5]))
+    later.insert(9, pltpu.make_async_copy(du_hbm, dgu.at[1], load_sem.at[7]))
+    held = [pltpu.make_async_copy(wgu, wgu, load_sem.at[5]), later[7], pltpu.make_async_copy(dgu, dgu, load_sem.at[7]), later[10]]
     for load in small + caches + later[:5]:
         load.start()
 
@@ -86,11 +97,11 @@
         inner = low * deep + (1 - low) * (3 - deep)
         line = [inner, 1 - inner, 2, 3]
         line = [low * at + (1 - low) * (3 - at) for at in line]
-        peers = [line[k // 2] * 2 + (side if k % 2 == 0 else 1 - side) for k in range(n_ep)]
+        away = [line[k // 2] * 2 + (side if k % 2 == 0 else 1 - side) for k in range(n_ep - 1, 0, -1)]
     else:
-        peers = [lax.rem(me + k, n_ep) for k in range(n_ep)]
-    sets = [list(range(4)), list(range(4, 8))] if n_ep == 8 else [list(range(n_ep))]
-    far_first = list(range(n_ep - 1, 0, -1))
+        away = [lax.rem(me + k, n_ep) for k in range(1, n_ep)]
+    rising = [k + (me <= k).astype(jnp.int32) for k in range(n_ep - 1)]
+    sets = block_sets(n_ep)
 
     contract = (((1,), (1,)), ((), ()))
 
@@ -116,7 +127,7 @@
     normed_one = rms(token_f, attn_gain_ref[...]).astype(bf16)
     small[2].wait()
     query_raw = jnp.dot(normed_one, wq[...], preferred_element_type=f32)
-    for load in small[3:10]:
+    for load in [both] + small[5:10]:
         load.wait()
     pair_raw = lax.dot_general(normed_one, wkv[...], contract, preferred_element_type=f32)
     gate_in = jnp.sum(normed_one.astype(f32) * forget_ref[...].astype(f32), axis=1, keepdims=True) + bias_ref[...]
@@ -216,46 +227,39 @@
     residual = (token_block + attn).astype(bf16)
     gathered[col, me] = residual
 
-    for k in far_first:
-        to_ep(gathered.at[col, me], gathered.at[col, me], ring_send, ring_recv.at[me], peers[k]).start()
+    for peer in away:
+        to_ep(gathered.at[col, me], gathered.at[col, me], ring_send, ring_recv.at[me], peer).start()
     if n_tp == 4:
-        across, beside = lax.rem(col + 2, 4), col + 1 - 2 * lax.rem(col, 2)
-        others = [across, lax.rem(col + 2, 4) + 1 - 2 * lax.rem(col, 2), beside]
-        relayed = [k for k in range(n_ep) if k < 0]
+        across = lax.rem(col + 2, 4)
+        others = [across, across + 1 - 2 * lax.rem(col, 2), col + 1 - 2 * lax.rem(col, 2)]
     else:
-        across, beside = col, col
         others = [lax.rem(col + d, n_tp) for d in range(1, n_tp)]
-        relayed = []
-
-    def to_other(block, slot, recv, other):
+
+    def fan(slot):
+        for other in others:
+            pltpu.make_async_remote_copy(
+                src_ref=gathered.at[col, slot], dst_ref=gathered.at[col, slot],
+                send_sem=fan_send, recv_sem=fan_recv.at[set_of(slot)],
+                device_id={"tp": other}, device_id_type=MESH).start()
+
+    def set_of(slot):
+        return sum((slot >= chosen[0]).astype(jnp.int32) for chosen in sets) - 1
+
+    def spread(n):
+        group = gathered.at[pl.ds(0, n_tp - 1), pl.ds(sets[n][0], len(sets[n]))]
         return pltpu.make_async_remote_copy(
-            src_ref=gathered.at[block, slot], dst_ref=gathered.at[block, slot],
-            send_sem=fan_send, recv_sem=recv, device_id={"tp": other}, device_id_type=MESH)
-
-    def arrive(k):
-        slot = peers[k]
-        if k > 0:
-            to_ep(gathered.at[col, slot], gathered.at[col, slot], ring_send, ring_recv.at[slot], slot).wait_recv()
-        if k in relayed:
-            to_other(col, slot, cross_recv.at[k], across).start()
-            to_other(col, slot, fan_recv.at[k], beside).start()
-        else:
-            for other in others:
-                to_other(col, slot, fan_recv.at[k], other).start()
-
-    def relay(k):
-        to_other(col, peers[k], cross_recv.at[k], across).wait_recv()
-        to_other(across, peers[k], fan_recv.at[k], beside).start()
-
-    def spread(k, blocks):
-        group = gathered.at[pl.ds(0, blocks), peers[k]]
-        return pltpu.make_async_remote_copy(
-            src_ref=group, dst_ref=group, send_sem=fan_send, recv_sem=fan_recv.at[k],
+            src_ref=group, dst_ref=group, send_sem=fan_send, recv_sem=fan_recv.at[n],
             device_id={"tp": others[0]}, device_id_type=MESH)
 
-    arrive(0)
+    fan(me)
     for load in later[1:5]:
         load.wait()
+    def token_lines(chosen):
+        return slice(chosen[0] * seq_rows, (chosen[-1] + 1) * seq_rows)
+
+    def slot_lines(chosen):
+        return slice(chosen[0] * cap, (chosen[-1] + 1) * cap)
+
     expert = me
     hit = jnp.zeros((1, batch), f32)
     weight_row = jnp.zeros((1, batch), f32)
@@ -266,38 +270,26 @@
     row_at = iota((batch, batch), 0)
     col_at = iota((batch, batch), 1)
     hits = jnp.broadcast_to(hit, (8, batch)).astype(bf16)
-    if len(sets) > 1:
-        lane = iota((1, batch), 1)
-        block = group_of(lane, seq_rows)
-        source = lane - block * seq_rows
-        for k in range(n_ep):
-            source = source + jnp.where(block == k, (peers[k] * seq_rows).astype(f32), 0.0)
-        turn = jnp.where(row_at == source, 1.0, 0.0)
-        hits = jnp.dot(hits, turn.astype(bf16), preferred_element_type=f32).astype(bf16)
-        weight_row = jnp.dot(
-            jnp.broadcast_to(weight_row, (8, batch)), turn,
-            precision=lax.Precision.HIGHEST, preferred_element_type=f32)[0:1]
     hit = hits[0:1].astype(f32)
     before = (row_at <= col_at) & (row_at >= group_of(col_at, seq_rows) * seq_rows)
     rank = jnp.dot(hits, before.astype(f32).astype(bf16), preferred_element_type=f32)[0:1]
     slot_of = jnp.where((hit > 0.5) & (rank < cap + 0.5), group_of(iota((1, batch), 1), seq_rows) * cap + rank - 1.0, -1.0)
     for n, chosen in enumerate(sets):
-        lines = len(chosen) * seq_rows
-        places = len(chosen) * cap
-        here = slot_of[:, n * lines:(n + 1) * lines]
-        pick = jnp.where(iota((places, lines), 0) + n * places == here, 1.0, 0.0)
-        pick_ref[n] = pick.astype(bf16)
-        place_ref[n] = pick.T.astype(bf16)
-        weight_ref[n] = jnp.sum((pick * weight_row[:, n * lines:(n + 1) * lines]).T, axis=1, keepdims=True)
+        lines, places = token_lines(chosen), slot_lines(chosen)
+        here = slot_of[:, lines]
+        size = len(chosen) * cap, len(chosen) * seq_rows
+        pick = jnp.where(iota(size, 0) + chosen[0] * cap == here, 1.0, 0.0)
+        pick_ref[n, 0:size[0], 0:size[1]] = pick.astype(bf16)
+        place_ref[n, 0:size[1], 0:size[0]] = pick.T.astype(bf16)
+        weight_ref[lines, :] = jnp.sum((pick * weight_row[:, lines]).T, axis=1, keepdims=True)
     shared_tiles = shared_ref[...].astype(f32)
     shared = jnp.concatenate([shared_tiles[i:i + 1] for i in range(width // 128)], axis=1)
 
-    def lines_of(k):
-        at = k * seq_rows if len(sets) > 1 else pl.multiple_of(peers[k] * seq_rows, 8)
-        return pl.ds(at, seq_rows)
+    def lines_of(slot):
+        return slice(slot * seq_rows, (slot + 1) * seq_rows)
 
     def normalize(k):
-        blocks = [gathered[t, peers[k]].astype(f32) for t in range(n_tp)]
+        blocks = [gathered[t, k].astype(f32) for t in range(n_tp)]
         squares = sum(jnp.sum(b * b, axis=1, keepdims=True) for b in blocks)
         scale = lax.rsqrt(squares / width + EPSILON)
         for t in range(n_tp):
@@ -305,28 +297,30 @@
                 blocks[t] * scale * gain_ref[:, t * span:(t + 1) * span])
 
     def expert_part(n, chosen):
-        lines = len(chosen) * seq_rows
-        rows = rows_f[n * lines:(n + 1) * lines, :].astype(bf16)
-        picked = jnp.dot(pick_ref[n], rows, preferred_element_type=f32).astype(bf16)
-        gate = jnp.dot(picked, wg[...], preferred_element_type=f32)
-        up = jnp.dot(picked, wu[...], preferred_element_type=f32)
+        rows = rows_f[token_lines(chosen), :].astype(bf16)
+        pick = pick_ref[n, 0:len(chosen) * cap, 0:len(chosen) * seq_rows]
+        picked = jnp.dot(pick, rows, preferred_element_type=f32).astype(bf16)
+        gate = jnp.dot(picked, wgu[0], preferred_element_type=f32)
+        up = jnp.dot(picked, wgu[1], preferred_element_type=f32)
         hidden = (gate / (1.0 + jnp.exp(-gate)) * up).astype(bf16)
         down = jnp.dot(hidden, wd[...], preferred_element_type=f32).astype(bf16)
+        places = slot_lines(chosen)
         for j in range(n_tp):
-            exp_out[n, j] = down[:, j * span:(j + 1) * span]
+            exp_out[j, places, :] = down[:, j * span:(j + 1) * span]
+        part = pl.ds(chosen[0] * cap, len(chosen) * cap)
         for d in sorted(range(1, n_tp), key=lambda d: d != 2):
             there = lax.rem(col + d, n_tp)
-            to_tp(exp_out.at[n, there], exp_in.at[n, col], exp_send.at[n], exp_recv.at[n], d).start()
-        exp_in[n, col] = exp_out[n, col]
+            to_tp(exp_out.at[there, part], exp_in.at[col, part], exp_send.at[n], exp_recv.at[n], d).start()
+        exp_in[col, places, :] = exp_out[col, places, :]
 
     def moves(n):
-        there = pl.ds(0, n_tp - 1)
-        return to_tp(exp_out.at[n, there], exp_in.at[n, there], exp_send.at[n], exp_recv.at[n], 1)
+        there = exp_in.at[pl.ds(0, n_tp - 1), pl.ds(sets[n][0] * cap, len(sets[n]) * cap)]
+        return to_tp(there, there, exp_send.at[n], exp_recv.at[n], 1)
 
     def dense(rows):
         rows = rows.astype(bf16)
-        gate = lax.dot_general(rows, dg[...], contract, preferred_element_type=f32)
-        up = lax.dot_general(rows, du[...], contract, preferred_element_type=f32)
+        gate = lax.dot_general(rows, dgu[0], contract, preferred_element_type=f32)
+        up = lax.dot_general(rows, dgu[1], contract, preferred_element_type=f32)
         hidden = (gate / (1.0 + jnp.exp(-gate)) * up).astype(bf16)
         mix = jnp.sum(rows.astype(f32) * shared, axis=1, keepdims=True)
         mix = 1.0 / (1.0 + jnp.exp(-mix))
@@ -334,30 +328,27 @@
 
     def finish(n, chosen):
         moves(n).wait_recv()
-        rows = exp_in[n, 0].astype(f32)
+        places, lines = slot_lines(chosen), token_lines(chosen)
+        rows = exp_in[0, places, :].astype(f32)
         for j in range(1, n_tp):
-            rows = rows + exp_in[n, j].astype(f32)
-        placed = jnp.dot(place_ref[n], rows.astype(bf16), preferred_element_type=f32) * weight_ref[n]
-        lines = len(chosen) * seq_rows
-        total[n * lines:(n + 1) * lines, :] = total[n * lines:(n + 1) * lines, :] + placed
-        for k in reversed(chosen):
-            if k > 0:
-                sum_out[k] = total[lines_of(k), :].astype(bf16)
-        for k in reversed(chosen):
-            if k > 0:
-                to_ep(sum_out.at[k], sum_in.at[me], sum_send, sum_recv.at[me], peers[k]).start()
-
-    for k in range(1, n_ep):
-        arrive(k)
-        if k - 4 in relayed:
-            relay(k - 4)
-    for load in later[5:]:
+            rows = rows + exp_in[j, places, :].astype(f32)
+        place = place_ref[n, 0:len(chosen) * seq_rows, 0:len(chosen) * cap]
+        placed = jnp.dot(place, rows.astype(bf16), preferred_element_type=f32) * weight_ref[lines, :]
+        total[lines, :] = total[lines, :] + placed
+        for slot in chosen:
+            sum_out[slot] = total[lines_of(slot), :].astype(bf16)
+        for slot in (chosen if 2 * n < len(sets) else reversed(chosen)):
+            @pl.when(slot != me)
+            def _():
+                to_ep(sum_out.at[slot], sum_in.at[me], sum_send, sum_recv, slot).start()
+
+    for slot in rising:
+        to_ep(gathered.at[col, slot], gathered.at[col, slot], ring_send, ring_recv.at[slot], slot).wait_recv()
+        fan(slot)
+    for load in held:
         load.wait()
     for n, chosen in enumerate(sets):
-        for k in chosen:
-            if k > n_ep - 1 - 4 and k in relayed:
-                relay(k)
-            spread(k, 2 if k in relayed else n_tp - 1).wait_recv()
+        spread(n).wait_recv()
         for k in chosen:
             normalize(k)
         expert_part(n, chosen)
@@ -371,20 +362,21 @@
             total[pl.ds(at, step), :] = dense(rows_f[pl.ds(at, step), :])
     for n, chosen in enumerate(sets):
         finish(n, chosen)
-    result = residual.astype(f32) + total[lines_of(0), :]
-    for k in range(1, n_ep):
-        slot = peers[k]
-        to_ep(sum_out.at[k], sum_in.at[slot], sum_send, sum_recv.at[slot], slot).wait_recv()
+    most = pl.ds(0, n_ep - 1)
+    result = residual.astype(f32) + total[pl.ds(pl.multiple_of(me * seq_rows, 8), seq_rows), :]
+    sums = to_ep(sum_in.at[most], sum_in.at[most], sum_send, sum_recv, away[0])
+    sums.wait_recv()
+    sum_in[me] = jnp.zeros_like(sum_in[me])
+    for slot in range(n_ep):
         result = result + sum_in[slot].astype(f32)
     out_ref[...] = result.astype(bf16)
     parts.wait_send()
-    others_of = gathered.at[0, pl.ds(0, n_ep - 1)]
-    to_ep(others_of, others_of, ring_send, ring_recv.at[0], peers[1]).wait_send()
-    for k in range(n_ep):
-        spread(k, n_tp - 1).wait_send()
+    to_ep(gathered.at[0, most], gathered.at[0, most], ring_send, ring_recv.at[0], away[0]).wait_send()
+    for n in range(len(sets)):
+        spread(n).wait_send()
     for n in range(len(sets)):
         moves(n).wait_send()
-    to_ep(sum_out.at[pl.ds(1, n_ep - 1)], sum_in.at[pl.ds(1, n_ep - 1)], sum_send, sum_recv.at[1], peers[1]).wait_send()
+    sums.wait_send()
 
 
 def layer_call(tokens, attn_gain, w_query, w_key, w_value, w_forget, forget_bias, query_gain, key_gain,
@@ -393,7 +385,8 @@
     n_ep, n_tp = lax.axis_size("ep"), lax.axis_size("tp")
     seq_rows, width = tokens.shape
     cap = max(2, min(seq_rows, 128 // n_ep))
-    n_sets = 2 if n_ep == 8 else 1
+    sets = block_sets(n_ep)
+    n_sets, most = len(sets), max(len(chosen) for chosen in sets)
     span = width // n_tp
     slots, batch = n_ep * cap, n_ep * seq_rows
     bf16, f32 = jnp.bfloat16, jnp.float32
@@ -423,32 +416,30 @@
             pltpu.VMEM((seq_rows,) + cache_pairs.shape[2:], bf16),
             pltpu.VMEM(w_output.shape, bf16),
             pltpu.VMEM((seq_rows, w_query.shape[1]), f32),
-            pltpu.VMEM(w_exp_gate.shape[1:], bf16),
-            pltpu.VMEM(w_exp_up.shape[1:], bf16),
+            pltpu.VMEM((2,) + w_exp_gate.shape[1:], bf16),
             pltpu.VMEM(w_exp_down.shape[1:], bf16),
-            pltpu.VMEM(w_dense_gate.shape, bf16),
-            pltpu.VMEM(w_dense_up.shape, bf16),
+            pltpu.VMEM((2,) + w_dense_gate.shape, bf16),
             pltpu.VMEM(w_dense_down.shape, bf16),
             pltpu.VMEM((n_tp, seq_rows, span), bf16),
             pltpu.VMEM((n_tp, seq_rows, span), bf16),
             pltpu.VMEM((n_tp, n_ep, seq_rows, span), bf16),
             pltpu.VMEM((batch, width), f32),
-            pltpu.VMEM((n_sets, slots // n_sets, batch // n_sets), bf16),
-            pltpu.VMEM((n_sets, batch // n_sets, slots // n_sets), bf16),
-            pltpu.VMEM((n_sets, batch // n_sets, 1), f32),
-            pltpu.VMEM((n_sets, n_tp, slots // n_sets, span), bf16),
-            pltpu.VMEM((n_sets, n_tp, slots // n_sets, span), bf16),
+            pltpu.VMEM((n_sets, most * cap, most * seq_rows), bf16),
+            pltpu.VMEM((n_sets, most * seq_rows, most * cap), bf16),
+            pltpu.VMEM((batch, 1), f32),
+            pltpu.VMEM((n_tp, slots, span), bf16),
+            pltpu.VMEM((n_tp, slots, span), bf16),
             pltpu.VMEM((batch, span), f32),
             pltpu.VMEM((n_ep, seq_rows, span), bf16),
             pltpu.VMEM((n_ep, seq_rows, span), bf16),
-            dma((11,)),
+            dma((10,)),
             dma((seq_rows // 8,)),
-            dma((11,)),
+            dma((9,)),
             dma, dma,
             dma, dma((n_ep,)),
-            dma, dma((n_ep,)), dma((n_ep,)),
+            dma, dma((n_sets,)),
             dma((n_sets,)), dma((n_sets,)),
-            dma, dma((n_ep,)),
+            dma, dma,
         ],
         compiler_params=pltpu.CompilerParams(
             collective_id=0, has_side_effects=True, vmem_limit_bytes=VMEM_BYTES),

time: 32 us -> 28.7 us (0.90)
  the two profiles are of different devices: /device:TPU:0 before, /device:TPU:17 now
where the time goes in v3:
time: 28.7 us; the launch traced here: 28.6 us
  Pallas kernels  27.3 us (95%)
  between operations  0.66 us (2%)
  local copies, waits for them, and re-layouts  0.6 us (2%)
    pallas_call x1, Pallas kernels, layer_call(): pl.pallas_call(functools.partial(whole_layer, n_ep, n_tp, cap), out_shape...  27.3 us
    unnamed x1, local copies, waits for them, and re-layouts  0.6 us

profile of v3, /device:TPU:17, one launch (start us, length us, event | category | flops | bytes accessed | tf_op | source)
XLA Modules:
  0.0 28.6 jit_solution(8221121239740514874)
XLA Ops:
  0.7 27.3 %whole_layer.1 = bf16[24,256]{1,0:T(8,128)(2,1)S(1)} custom-call(bf16[24,1024]{1,0:T(8,128)(2,1)} %tokens_hbm.1, f32[1,1024]{1,0:T(1,128)} %bitcast.15, f32[1,64]{1,0:T(1,128)} %bitcast.21, f32[1,64]{1,0:T(1,128)} %bitcast.22, bf16[1,1024]{1,0:T(2,128)(2,1)} %bitcast.16, f32[1,1]{1,0:T(1,128)} %bitcast.12.bias_hbm, s32[1,24]{1,0:T(1,128)} %bitcast.23, ...), custom_call_target="tpu_custom_call" | custom-call | tf_op jit(solution)/shard_map/whole_layer/pallas_call | solution.py:396
  28.0 0.6 %copy.25 = bf16[24,256]{1,0:T(8,128)(2,1)} copy(bf16[24,256]{1,0:T(8,128)(2,1)S(1)} %whole_layer.1) | data formatting | bytes 24576

commit v4 on v3

--- a/solution.py
+++ b/solution.py
@@ -14,7 +14,7 @@
 
 def block_sets(n_ep):
     if n_ep == 8:
-        return [[0, 1], [2, 3], [4, 5, 6, 7]]
+        return [[0], [1, 2, 3], [4, 5, 6, 7]]
     return [list(range(n_ep))]
 
 
@@ -185,6 +185,10 @@
         inverse = 1.0 / (jnp.sum(past, axis=1, keepdims=True) + own)
         prob = (past * inverse).astype(bf16)
         own = rounded(own * inverse)
+        return prob, own
+
+    def gather_values(i, prob, own):
+        lines = slice(i * eight, (i + 1) * eight)
         values = jnp.concatenate([cache[i * eight + (b ^ 1), :, head:2 * head] for b in range(eight)], axis=1)
         wide = jnp.dot(prob, values, preferred_element_type=f32)
         mixes = []
@@ -195,17 +199,21 @@
         for a in range(heads // 2):
             mixed[lines, lanes * a:lanes * (a + 1)] = jnp.where(left_eight, mixes[2 * a], mixes[2 * a + 1])
 
-    score = None
-    for i in range(seq_rows // eight):
+    count = seq_rows // eight
+    score, prob = {}, {}
+    for i in range(count):
         for load in caches[i * eight // bunch:(i + 1) * eight // bunch]:
             load.wait()
-        ahead = score_of(i)
-        if score is not None:
-            attend(i - 1, score)
-        score = ahead
+        if i > 0:
+            prob[i - 1] = attend(i - 1, score[i - 1])
+        score[i] = score_of(i)
+        if i > 1:
+            gather_values(i - 2, *prob[i - 2])
+    prob[count - 1] = attend(count - 1, score[count - 1])
+    for i in range(max(count - 2, 0), count):
+        gather_values(i, *prob[i])
     for load in later[5:]:
         load.start()
-    attend(seq_rows // eight - 1, score)
     head_mix = mixed[...].astype(bf16)
     later[0].wait()
 
@@ -296,14 +304,24 @@
             rows_f[lines_of(k), t * span:(t + 1) * span] = (
                 blocks[t] * scale * gain_ref[:, t * span:(t + 1) * span])
 
-    def expert_part(n, chosen):
+    def prepare(n):
+        chosen = sets[n]
+        for k in chosen:
+            normalize(k)
         rows = rows_f[token_lines(chosen), :].astype(bf16)
         pick = pick_ref[n, 0:len(chosen) * cap, 0:len(chosen) * seq_rows]
-        picked = jnp.dot(pick, rows, preferred_element_type=f32).astype(bf16)
+        return jnp.dot(pick, rows, preferred_element_type=f32).astype(bf16)
+
+    def hidden_of(picked):
         gate = jnp.dot(picked, wgu[0], preferred_element_type=f32)
         up = jnp.dot(picked, wgu[1], preferred_element_type=f32)
-        hidden = (gate / (1.0 + jnp.exp(-gate)) * up).astype(bf16)
-        down = jnp.dot(hidden, wd[...], preferred_element_type=f32).astype(bf16)
+        return (gate / (1.0 + jnp.exp(-gate)) * up).astype(bf16)
+
+    def down_of(hidden):
+        return jnp.dot(hidden, wd[...], preferred_element_type=f32).astype(bf16)
+
+    def send_moves(n, down):
+        chosen = sets[n]
         places = slot_lines(chosen)
         for j in range(n_tp):
             exp_out[j, places, :] = down[:, j * span:(j + 1) * span]
@@ -347,11 +365,16 @@
         fan(slot)
     for load in held:
         load.wait()
-    for n, chosen in enumerate(sets):
-        spread(n).wait_recv()
-        for k in chosen:
-            normalize(k)
-        expert_part(n, chosen)
+    spread(0).wait_recv()
+    picked = prepare(0)
+    for n in range(len(sets)):
+        hidden = hidden_of(picked)
+        if n + 1 < len(sets):
+            spread(n + 1).wait_recv()
+        down = down_of(hidden)
+        if n + 1 < len(sets):
+            picked = prepare(n + 1)
+        send_moves(n, down)
     step = seq_rows * 8 if n_ep % 8 == 0 else batch
     if step == batch:
         total[...] = dense(rows_f[...])

time: 28.7 us -> 27.9 us (0.972)
  the two profiles are of different devices: /device:TPU:17 before, /device:TPU:0 now
where the time goes in v4:
time: 27.9 us; the launch traced here: 27.7 us
  Pallas kernels  26.5 us (95%)
  between operations  0.66 us (2%)
  local copies, waits for them, and re-layouts  0.6 us (2%)
    pallas_call x1, Pallas kernels, layer_call(): pl.pallas_call(functools.partial(whole_layer, n_ep, n_tp, cap), out_shape...  26.5 us
    unnamed x1, local copies, waits for them, and re-layouts  0.6 us

profile of v4, /device:TPU:0, one launch (start us, length us, event | category | flops | bytes accessed | tf_op | source)
XLA Modules:
  0.0 27.7 jit_solution(17547605940321886103)
XLA Ops:
  0.7 26.5 %whole_layer.1 = bf16[24,256]{1,0:T(8,128)(2,1)S(1)} custom-call(bf16[24,1024]{1,0:T(8,128)(2,1)} %tokens_hbm.1, f32[1,1024]{1,0:T(1,128)} %bitcast.15, f32[1,64]{1,0:T(1,128)} %bitcast.21, f32[1,64]{1,0:T(1,128)} %bitcast.22, bf16[1,1024]{1,0:T(2,128)(2,1)} %bitcast.16, f32[1,1]{1,0:T(1,128)} %bitcast.12.bias_hbm, s32[1,24]{1,0:T(1,128)} %bitcast.23, ...), custom_call_target="tpu_custom_call" | custom-call | tf_op jit(solution)/shard_map/whole_layer/pallas_call | solution.py:419
  27.1 0.6 %copy.25 = bf16[24,256]{1,0:T(8,128)(2,1)} copy(bf16[24,256]{1,0:T(8,128)(2,1)S(1)} %whole_layer.1) | data formatting | bytes 24576

commit v5 on v4

--- a/solution.py
+++ b/solution.py
@@ -29,7 +29,7 @@
     gain_ref, ids_ref, route_ref, shared_ref,
     wq, wkv, cum, cache, wo_ref, mixed,
     wgu, wd, dgu, dd,
-    part_out, part_in, gathered, rows_f, pick_ref, place_ref, weight_ref, exp_out, exp_in, total, sum_out, sum_in,
+    part_out, part_in, gathered, rows_f, pick_ref, place_ref, weight_ref, mix_ref, exp_out, exp_in, total, sum_out, sum_in,
     small_sem, attn_sem, load_sem, part_send, part_recv, ring_send, ring_recv, fan_send, fan_recv,
     exp_send, exp_recv, sum_send, sum_recv,
 ):
@@ -207,10 +207,8 @@
         if i > 0:
             prob[i - 1] = attend(i - 1, score[i - 1])
         score[i] = score_of(i)
-        if i > 1:
-            gather_values(i - 2, *prob[i - 2])
     prob[count - 1] = attend(count - 1, score[count - 1])
-    for i in range(max(count - 2, 0), count):
+    for i in range(count):
         gather_values(i, *prob[i])
     for load in later[5:]:
         load.start()
@@ -221,7 +219,7 @@
     for j in range(n_tp):
         part_out[j] = partial[:, j * span:(j + 1) * span]
     pl.semaphore_wait(barrier, n_ep + n_tp - 2)
-    for d in range(1, n_tp):
+    for d in sorted(range(1, n_tp), key=lambda d: d != 2):
         there = lax.rem(col + d, n_tp)
         to_tp(part_out.at[there], part_in.at[col], part_send, part_recv, d).start()
     some = pl.ds(0, n_tp - 1)
@@ -309,6 +307,8 @@
         for k in chosen:
             normalize(k)
         rows = rows_f[token_lines(chosen), :].astype(bf16)
+        mix = jnp.sum(rows.astype(f32) * shared, axis=1, keepdims=True)
+        mix_ref[token_lines(chosen), :] = 1.0 / (1.0 + jnp.exp(-mix))
         pick = pick_ref[n, 0:len(chosen) * cap, 0:len(chosen) * seq_rows]
         return jnp.dot(pick, rows, preferred_element_type=f32).astype(bf16)
 
@@ -340,9 +340,7 @@
         gate = lax.dot_general(rows, dgu[0], contract, preferred_element_type=f32)
         up = lax.dot_general(rows, dgu[1], contract, preferred_element_type=f32)
         hidden = (gate / (1.0 + jnp.exp(-gate)) * up).astype(bf16)
-        mix = jnp.sum(rows.astype(f32) * shared, axis=1, keepdims=True)
-        mix = 1.0 / (1.0 + jnp.exp(-mix))
-        return mix * jnp.dot(hidden, dd[...], preferred_element_type=f32)
+        return jnp.dot(hidden, dd[...], preferred_element_type=f32)
 
     def finish(n, chosen):
         moves(n).wait_recv()
@@ -369,20 +367,23 @@
     picked = prepare(0)
     for n in range(len(sets)):
         hidden = hidden_of(picked)
-        if n + 1 < len(sets):
+        if n + 1 < len(sets) and n > 0:
             spread(n + 1).wait_recv()
         down = down_of(hidden)
-        if n + 1 < len(sets):
+        if n + 1 < len(sets) and n > 0:
             picked = prepare(n + 1)
         send_moves(n, down)
+        if n + 1 < len(sets) and n == 0:
+            spread(n + 1).wait_recv()
+            picked = prepare(n + 1)
     step = seq_rows * 8 if n_ep % 8 == 0 else batch
     if step == batch:
-        total[...] = dense(rows_f[...])
+        total[...] = mix_ref[...] * dense(rows_f[...])
     else:
         @pl.loop(0, batch // step)
         def _(i):
             at = pl.multiple_of(i * step, step)
-            total[pl.ds(at, step), :] = dense(rows_f[pl.ds(at, step), :])
+            total[pl.ds(at, step), :] = mix_ref[pl.ds(at, step), :] * dense(rows_f[pl.ds(at, step), :])
     for n, chosen in enumerate(sets):
         finish(n, chosen)
     most = pl.ds(0, n_ep - 1)
@@ -450,6 +451,7 @@
             pltpu.VMEM((n_sets, most * cap, most * seq_rows), bf16),
             pltpu.VMEM((n_sets, most * seq_rows, most * cap), bf16),
             pltpu.VMEM((batch, 1), f32),
+            pltpu.VMEM((batch, 1), f32),
             pltpu.VMEM((n_tp, slots, span), bf16),
             pltpu.VMEM((n_tp, slots, span), bf16),
             pltpu.VMEM((batch, span), f32),

time: 27.9 us -> 27.7 us (level)
  Pallas kernels: 26.5 us -> 26.2 us
where the time goes in v5:
time: 27.7 us; the launch traced here: 27.5 us
  Pallas kernels  26.2 us (95%)
  between operations  0.66 us (2%)
  local copies, waits for them, and re-layouts  0.6 us (2%)
    pallas_call x1, Pallas kernels, layer_call(): pl.pallas_call(functools.partial(whole_layer, n_ep, n_tp, cap), out_shape...  26.2 us
    unnamed x1, local copies, waits for them, and re-layouts  0.6 us

profile of v5, /device:TPU:0, one launch (start us, length us, event | category | flops | bytes accessed | tf_op | source)
XLA Modules:
  0.0 27.5 jit_solution(11354416738716034381)
XLA Ops:
  0.7 26.2 %whole_layer.1 = bf16[24,256]{1,0:T(8,128)(2,1)S(1)} custom-call(bf16[24,1024]{1,0:T(8,128)(2,1)} %tokens_hbm.1, f32[1,1024]{1,0:T(1,128)} %bitcast.15, f32[1,64]{1,0:T(1,128)} %bitcast.21, f32[1,64]{1,0:T(1,128)} %bitcast.22, bf16[1,1024]{1,0:T(2,128)(2,1)} %bitcast.16, f32[1,1]{1,0:T(1,128)} %bitcast.12.bias_hbm, s32[1,24]{1,0:T(1,128)} %bitcast.23, ...), custom_call_target="tpu_custom_call" | custom-call | tf_op jit(solution)/shard_map/whole_layer/pallas_call | solution.py:420
  26.9 0.6 %copy.25 = bf16[24,256]{1,0:T(8,128)(2,1)} copy(bf16[24,256]{1,0:T(8,128)(2,1)S(1)} %whole_layer.1) | data formatting | bytes 24576
